TPU v7x, 32 devices: a whole 2x2x4 slice. The times are simulated.
32 devices in a mesh: rep: 2 (over x), fs: 8 (over z, y), tp: 2 (over core).
Axes of the slice: x: 2, y: 2, z: 4, core: 2. Of those that a mesh axis runs over, the one named last changes fastest.
Arguments:
- tokens: bfloat16 [16384, 2048], P(('rep', 'fs', 'tp')), may hold values from -6 to 6
- mix_gain: float32 [2048], replicated, may hold values from 0.1 to 1.9
- query_weight: bfloat16 [2048, 2048], P('fs', 'tp'), may hold values from -0.125 to 0.125
- key_weight: bfloat16 [2048, 2048], P('fs', 'tp'), may hold values from -0.125 to 0.125
- value_weight: bfloat16 [2048, 2048], P('fs', 'tp'), may hold values from -0.125 to 0.125
- gate_weight: bfloat16 [2048, 2048], P('fs', 'tp'), may hold values from -0.125 to 0.125
- out_weight: bfloat16 [2048, 2048], P('fs', 'tp'), may hold values from -0.125 to 0.125
- head_gain: float32 [2048], replicated, may hold values from 0.1 to 1.9
- channel_gain: float32 [2048], replicated, may hold values from 0.1 to 1.9
- inner_gate: bfloat16 [2048, 6144], P('fs', 'tp'), may hold values from -0.125 to 0.125
- inner_lift: bfloat16 [2048, 6144], P('fs', 'tp'), may hold values from -0.125 to 0.125
- inner_down: bfloat16 [2048, 6144], P('fs', 'tp'), may hold values from -0.078125 to 0.078125
- filter_taps: float32 [3, 6144], replicated, may hold values from -3.5 to 3.5
- filter_bias: float32 [6144], replicated, may hold values from -3 to 3
Outputs:
- result: bfloat16 [16384, 2048], P(('rep', 'fs', 'tp'))
All inputs are finite; a program needn't handle non-finite values.
Results may differ from a plain program's by a relative error of at most 0.017.
Values may be sent and summed in bfloat16 or wider, within the bound.
A program may use at most 128 MiB of HBM per device.

v0:
```python
import jax
import jax.numpy as jnp
from jax import lax
from jax.experimental import pallas as pl
from jax.experimental.pallas import tpu as pltpu
from jax.sharding import PartitionSpec as P


HEAD_DIM = 256
BLOCK = 128
TAPS = 3


norm_eps = 1e-06
head_eps = 1.0
rope_base = 10000.0


def rms_scale(features, gain_row):
    mean_square = jnp.mean(features * features, axis=-1, keepdims=True)
    return features * lax.rsqrt(mean_square + norm_eps) * gain_row


def rotate(heads_in, positions):
    half_width = heads_in.shape[-1] // 2
    inverse = rope_base ** (-jnp.arange(half_width, dtype=jnp.float32) / half_width)
    angles = positions[:, None] * inverse[None, :]
    cosine = jnp.cos(angles)[:, None, :]
    sine_part = jnp.sin(angles)[:, None, :]
    front_half = heads_in[..., :half_width]
    back_half = heads_in[..., half_width:]
    return jnp.concatenate(
        [front_half * cosine - back_half * sine_part, front_half * sine_part + back_half * cosine],
        axis=-1,
    )


def retain(queries, key_rows, value_rows, log_gamma, span):
    full_length, head_count, head_width = queries.shape
    blocks = full_length // span
    offsets = jnp.arange(span, dtype=jnp.float32)
    distance = offsets[:, None] - offsets[None, :]
    inside_segment_decay = jnp.where(
        distance[None] >= 0,
        jnp.exp(jnp.maximum(distance, 0.0)[None] * log_gamma[:, None, None]),
        0.0,
    )
    query_decay = jnp.exp((offsets[None, :] + 1.0) * log_gamma[:, None])
    key_decay_factor = jnp.exp((span - 1.0 - offsets[None, :]) * log_gamma[:, None])
    span_decay = jnp.exp(span * log_gamma)

    def to_spans(array):
        return array.reshape(blocks, span, head_count, head_width).transpose(0, 2, 1, 3)

    def advance(carry_state, inputs):
        query_segment, key_segment, value_span = inputs
        attention_scores = (
            jnp.einsum(
                "pol,pel->poe", query_segment, key_segment, preferred_element_type=jnp.float32
            )
            * inside_segment_decay
        )
        span_weights = attention_scores.astype(jnp.bfloat16)
        within_span = jnp.einsum(
            "hnm,hme->hne", span_weights, value_span, preferred_element_type=jnp.float32
        )
        carried = (
            jnp.einsum(
                "hnd,hde->hne",
                query_segment.astype(jnp.float32),
                carry_state,
                precision=lax.Precision.HIGHEST,
            )
            * query_decay[:, :, None]
        )
        state_update = jnp.einsum(
            "lqc,lqu->lcu",
            key_segment.astype(jnp.float32) * key_decay_factor[:, :, None],
            value_span.astype(jnp.float32),
            precision=lax.Precision.HIGHEST,
        )
        return (carry_state * span_decay[:, None, None] + state_update, within_span + carried)

    initial = jnp.zeros((head_count, head_width, head_width), jnp.float32)
    _, outputs = lax.scan(
        advance, initial, (to_spans(queries), to_spans(key_rows), to_spans(value_rows))
    )
    return outputs.transpose(0, 2, 1, 3).reshape(full_length, head_count, head_width)


def transposed_product(rows_in, weight):
    return lax.dot_general(
        rows_in, weight, (((1,), (1,)), ((), ())), preferred_element_type=jnp.float32
    )


def shift_pairs(groups, step):
    return [(source, (source + step) % groups) for source in range(groups)]


def gather_rows(rows, groups, index):
    rows_dev = rows.shape[0]
    whole = jnp.zeros((rows_dev * groups,) + rows.shape[1:], rows.dtype)
    whole = lax.dynamic_update_slice_in_dim(whole, rows, index * rows_dev, 0)
    for step in range(1, groups):
        arrived = lax.ppermute(rows, "tp", shift_pairs(groups, step))
        owner = (index - step + groups) % groups
        whole = lax.dynamic_update_slice_in_dim(whole, arrived, owner * rows_dev, 0)
    return whole


def sum_groups(partial, groups):
    total = partial.astype(jnp.float32)
    for step in range(1, groups):
        arrived = lax.ppermute(partial, "tp", shift_pairs(groups, step))
        total = total + arrived.astype(jnp.float32)
    return total


def scatter_groups(partial, groups, index):
    rows_dev = partial.shape[0] // groups
    total = lax.dynamic_slice_in_dim(partial, index * rows_dev, rows_dev, 0).astype(jnp.float32)
    for step in range(1, groups):
        target = (index + step) % groups
        leaving = lax.dynamic_slice_in_dim(partial, target * rows_dev, rows_dev, 0)
        arrived = lax.ppermute(leaving, "tp", shift_pairs(groups, step))
        total = total + arrived.astype(jnp.float32)
    return total


def shared_width(columns, unit, numerator, denominator):
    if lax.axis_size("rep") != 2:
        return 0
    return (columns // unit) * numerator // denominator * unit


def column_pieces(array, width):
    columns = array.shape[-1]
    if width == 0:
        return [array]
    rep_index = lax.axis_index("rep")
    pieces = [lax.dynamic_slice_in_dim(array, rep_index * (columns - width), width, array.ndim - 1)]
    if columns > 2 * width:
        pieces.append(array[..., width : columns - width])
    pieces.append(
        lax.dynamic_slice_in_dim(
            array, (1 - rep_index) * (columns - width), width, array.ndim - 1
        )
    )
    return pieces


def gather_weights(weights, width):
    columns = weights[0].shape[1]
    if width == 0:
        return [[lax.all_gather(weight, "fs", axis=0, tiled=True)] for weight in weights]
    rep_index = lax.axis_index("rep")
    start = rep_index * (columns - width)
    count = len(weights)

    def cut(whole):
        each = whole.shape[1] // count
        return [whole[:, order * each : (order + 1) * each] for order in range(count)]

    own = join([lax.dynamic_slice_in_dim(weight, start, width, 1) for weight in weights])
    first = lax.all_gather(own, "fs", axis=0, tiled=True)
    pieces = [cut(first)]
    if columns > 2 * width:
        common = join([weight[:, width : columns - width] for weight in weights])
        pieces.append(cut(lax.all_gather(common, "fs", axis=0, tiled=True)))
    pieces.append(cut(lax.ppermute(first, "rep", [(0, 1), (1, 0)])))
    return [list(each) for each in zip(*pieces)]


def product(rows_in, weight):
    return jnp.dot(rows_in, weight, preferred_element_type=jnp.float32).astype(jnp.bfloat16)


def join(pieces):
    return pieces[0] if len(pieces) == 1 else jnp.concatenate(pieces, axis=-1)


def shards_any(
    tokens,
    mix_gain,
    query_weight,
    key_weight,
    value_weight,
    gate_weight,
    out_weight,
    head_gain,
    channel_gain,
    inner_gate,
    inner_lift,
    inner_down,
    filter_taps,
    filter_bias,
):
    tp_index = lax.axis_index("tp")
    groups = lax.axis_size("tp")
    rows_dev = tokens.shape[0]
    cols_dev = query_weight.shape[1]
    hidden_dev = inner_gate.shape[1]
    heads_dev = cols_dev // HEAD_DIM
    full_length = rows_dev * groups
    head_width = shared_width(cols_dev, HEAD_DIM, 1, 2)
    hidden_width = shared_width(hidden_dev, 128, 1, 3)
    query_set, key_set = gather_weights([query_weight, key_weight], head_width)
    value_set, gate_set = gather_weights([value_weight, gate_weight], head_width)
    (out_set,) = gather_weights([out_weight], head_width)
    inner_gate_set, inner_lift_set = gather_weights([inner_gate, inner_lift], hidden_width)
    (down_set,) = gather_weights([inner_down], hidden_width)
    whole_tokens = gather_rows(tokens, groups, tp_index)
    normed_whole = lax.optimization_barrier(
        rms_scale(whole_tokens.astype(jnp.float32), mix_gain).astype(jnp.bfloat16)
    )
    queries = join([product(normed_whole, piece) for piece in query_set])
    key_rows = join([product(normed_whole, piece) for piece in key_set])
    value_rows = join([product(normed_whole, piece) for piece in value_set])
    gate_in = join([product(normed_whole, piece) for piece in gate_set])
    positions = jnp.arange(full_length, dtype=jnp.float32)
    q_rot = (
        rotate(queries.astype(jnp.float32).reshape(full_length, heads_dev, HEAD_DIM), positions)
        * HEAD_DIM ** (-0.5)
    ).astype(jnp.bfloat16)
    k_rot = rotate(
        key_rows.astype(jnp.float32).reshape(full_length, heads_dev, HEAD_DIM), positions
    ).astype(jnp.bfloat16)
    head_order = join(
        column_pieces(jnp.arange(heads_dev, dtype=jnp.int32), head_width // HEAD_DIM)
    )
    head_ids = (tp_index * heads_dev + head_order).astype(jnp.float32)
    log_gamma = jnp.log(1.0 - 2.0 ** (-5.0 - head_ids))
    retained = retain(
        q_rot, k_rot, value_rows.reshape(full_length, heads_dev, HEAD_DIM), log_gamma, BLOCK
    )
    mean_square = jnp.mean(retained * retained, axis=-1, keepdims=True)
    gain_dev = lax.dynamic_slice_in_dim(head_gain, tp_index * cols_dev, cols_dev, 0)
    gain_dev = join(column_pieces(gain_dev, head_width))
    head_normed = (retained * lax.rsqrt(mean_square + head_eps)).reshape(
        full_length, cols_dev
    ) * gain_dev
    mixed = (jax.nn.silu(gate_in.astype(jnp.float32)) * head_normed).astype(jnp.bfloat16)
    out_product = 0.0
    column = 0
    for piece in out_set:
        part = mixed[:, column : column + piece.shape[1]]
        out_product = out_product + transposed_product(part, piece)
        column += piece.shape[1]
    mixer_whole = sum_groups(out_product.astype(jnp.bfloat16), groups)
    middle_whole = whole_tokens.astype(jnp.float32) + mixer_whole
    normed_mid = lax.optimization_barrier(
        rms_scale(middle_whole, channel_gain).astype(jnp.bfloat16)
    )
    middle = lax.dynamic_slice_in_dim(middle_whole, tp_index * rows_dev, rows_dev, 0)
    taps_dev = lax.dynamic_slice_in_dim(filter_taps, tp_index * hidden_dev, hidden_dev, 1)
    bias_dev = lax.dynamic_slice_in_dim(filter_bias, tp_index * hidden_dev, hidden_dev, 0)
    taps_set = column_pieces(taps_dev, hidden_width)
    bias_set = column_pieces(bias_dev, hidden_width)
    down_product = 0.0
    for gate_piece, lift_piece, down_piece, taps_piece, bias_piece in zip(
        inner_gate_set, inner_lift_set, down_set, taps_set, bias_set
    ):
        gate_pre = product(normed_mid, gate_piece)
        lifted = product(normed_mid, lift_piece)
        padded = jnp.pad(gate_pre, ((TAPS - 1, 0), (0, 0)))
        filtered = bias_piece[None, :]
        for offset in range(TAPS):
            shifted = padded[offset : offset + full_length].astype(jnp.float32)
            filtered = filtered + shifted * taps_piece[offset][None, :]
        hidden = (jax.nn.silu(filtered) * lifted.astype(jnp.float32)).astype(jnp.bfloat16)
        down_product = down_product + transposed_product(hidden, down_piece)
    outcome = middle + scatter_groups(down_product.astype(jnp.bfloat16), groups, tp_index)
    return outcome.astype(jnp.bfloat16)


def ring_pairs(count):
    order = list(range(0, count, 2)) + list(range(count - 1, 0, -2))
    return order, [(order[at], order[(at + 1) % count]) for at in range(count)]


def after(array, *earlier):
    return lax.optimization_barrier((array,) + earlier)[0]


class Ring:
    def __init__(self, shard, count, far_way):
        _, ahead = ring_pairs(count)
        behind = [(target, source) for source, target in ahead]
        self.blocks = {0: shard}
        self.hops = []
        up = down = shard
        for step in range(1, count // 2 + 1):
            arrived = []
            for way in ways(step, count, far_way):
                if way == "up":
                    up = lax.ppermute(up, "fs", ahead)
                    self.blocks[count - step] = up
                    arrived.append(up)
                else:
                    down = lax.ppermute(down, "fs", behind)
                    self.blocks[step] = down
                    arrived.append(down)
            self.hops.append(tuple(arrived))

    def parts(self, distances):
        return [self.blocks[at] for at in distances]


def ways(step, count, far_way):
    return ("up", "down") if step < count // 2 else (far_way,)


FAR_WAY = {"ra": "up", "rb": "down", "rg": "up", "rl": "down", "rc": "up", "rd": "down"}


def swap(array, axis):
    return lax.ppermute(array, axis, [(0, 1), (1, 0)])


def retain_kernel(
    swapped_ref,
    log_gamma_ref,
    query_ref,
    key_ref,
    value_ref,
    gate_ref,
    cosine_ref,
    sine_ref,
    gain_ref,
    mixed_ref,
):
    log_gamma = log_gamma_ref[pl.program_id(0)]
    length, width = query_ref.shape
    late = swapped_ref[0] * (length // 2)
    half = width // 2
    span = BLOCK
    rows = lax.broadcasted_iota(jnp.int32, (span, span), 0)
    columns = lax.broadcasted_iota(jnp.int32, (span, span), 1)
    distance = (rows - columns).astype(jnp.float32)
    inside = jnp.where(distance >= 0, jnp.exp(jnp.maximum(distance, 0.0) * log_gamma), 0.0)
    offsets = lax.broadcasted_iota(jnp.int32, (span, width), 0).astype(jnp.float32)
    query_decay = jnp.exp((offsets + 1.0) * log_gamma)
    key_decay = jnp.exp((span - 1.0 - offsets) * log_gamma)
    span_decay = jnp.exp(jnp.full((width, width), span, jnp.float32) * log_gamma)
    gain = gain_ref[...]

    def turn(ref, at, stored, scale):
        rows_in = ref[stored, :].astype(jnp.float32)
        front, back = rows_in[:, :half], rows_in[:, half:]
        cosine = cosine_ref[pl.ds(at, span), :]
        sine = sine_ref[pl.ds(at, span), :]
        turned = jnp.concatenate(
            [front * cosine - back * sine, front * sine + back * cosine], axis=-1
        )
        return (turned * scale).astype(jnp.bfloat16)

    def both(wide):
        high = wide.astype(jnp.bfloat16)
        return high, (wide - high.astype(jnp.float32)).astype(jnp.bfloat16)

    def dot(left, right, left_axis, right_axis):
        return lax.dot_general(
            left,
            right,
            (((left_axis,), (right_axis,)), ((), ())),
            preferred_element_type=jnp.float32,
        )

    state = jnp.zeros((width, width), jnp.float32)
    for block in range(length // span):
        at = block * span
        first = at + late if at < length // 2 else at - late
        stored = pl.ds(pl.multiple_of(first, span), span)
        query = turn(query_ref, at, stored, HEAD_DIM ** (-0.5))
        key = turn(key_ref, at, stored, 1.0)
        value = value_ref[stored, :]
        weights = (dot(query, key, 1, 1) * inside).astype(jnp.bfloat16)
        retained = dot(weights, value, 1, 0)
        if block > 0:
            high, low = both(state)
            retained = retained + (dot(query, high, 1, 0) + dot(query, low, 1, 0)) * query_decay
        if block < length // span - 1:
            high, low = both(key.astype(jnp.float32) * key_decay)
            added = dot(high, value, 0, 0) + dot(low, value, 0, 0)
            state = state * span_decay + added
        mean_square = jnp.mean(retained * retained, axis=-1, keepdims=True)
        normed = retained * lax.rsqrt(mean_square + head_eps) * gain
        gate = gate_ref[stored, :].astype(jnp.float32)
        mixed_ref[stored, :] = (gate * jax.nn.sigmoid(gate) * normed).astype(jnp.bfloat16)


def mix_heads(query_key, value_gate, cosine, sine, gain, log_gamma, swapped):
    length, columns = value_gate.shape[0], query_key.shape[1] // 2
    heads = columns // HEAD_DIM
    front = pl.BlockSpec((length, HEAD_DIM), lambda head, *_: (0, head))
    back = pl.BlockSpec((length, HEAD_DIM), lambda head, *_: (0, head + heads))
    table = pl.BlockSpec((length, HEAD_DIM // 2), lambda head, *_: (0, 0))
    return pl.pallas_call(
        retain_kernel,
        out_shape=jax.ShapeDtypeStruct((length, columns), jnp.bfloat16),
        grid_spec=pltpu.PrefetchScalarGridSpec(
            num_scalar_prefetch=2,
            grid=(heads,),
            in_specs=[front, back, front, back, table, table]
            + [pl.BlockSpec((1, HEAD_DIM), lambda head, *_: (0, head))],
            out_specs=front,
        ),
        compiler_params=pltpu.CompilerParams(vmem_limit_bytes=VMEM_LIMIT),
        cost_estimate=pl.CostEstimate(
            flops=length * columns * (4 * BLOCK + 8 * HEAD_DIM) * 4,
            bytes_accessed=length * columns * 10,
            transcendentals=length * columns,
        ),
    )(swapped, log_gamma, query_key, query_key, value_gate, value_gate, cosine, sine, gain.reshape(1, -1))


VMEM_LIMIT = 26 * 2**20


def stacked(refs):
    return jnp.concatenate([ref[...] for ref in refs], axis=0)


def whole_block(array):
    return pl.BlockSpec(
        array.shape, lambda at: (0,) * array.ndim, pipeline_mode=pl.Buffered(1)
    )


def strip(array, width):
    return pl.BlockSpec((array.shape[0], width), lambda at: (0, at))


def project_rows(row_parts, weight_blocks, columns, width=256):
    count = len(row_parts)
    part_rows, depth = row_parts[0].shape
    width = min(width, columns)

    def body(*refs):
        weight = stacked(refs[count:-1])
        for at in range(count):
            refs[-1][pl.ds(at * part_rows, part_rows), :] = jnp.dot(
                refs[at][...], weight, preferred_element_type=jnp.float32
            ).astype(jnp.bfloat16)

    return pl.pallas_call(
        body,
        out_shape=jax.ShapeDtypeStruct((count * part_rows, columns), jnp.bfloat16),
        grid=(columns // width,),
        in_specs=[whole_block(part) for part in row_parts]
        + [strip(block, width) for block in weight_blocks],
        out_specs=pl.BlockSpec((count * part_rows, width), lambda at: (0, at)),
        compiler_params=pltpu.CompilerParams(vmem_limit_bytes=VMEM_LIMIT),
        cost_estimate=pl.CostEstimate(
            flops=2 * count * part_rows * depth * columns,
            bytes_accessed=2 * (count * part_rows * (depth + columns) + depth * columns),
            transcendentals=0,
        ),
    )(*row_parts, *weight_blocks)


def project_back(depth_parts, weight_blocks, first_strip=0, tile=256):
    count = len(depth_parts)
    rows, strip_depth = depth_parts[0].shape
    columns = sum(block.shape[0] for block in weight_blocks)
    part_rows = rows // 2
    tiles = part_rows // tile
    first = first_strip // count

    def body(*refs):
        rows_in = jnp.concatenate([ref[...] for ref in refs[:count]], axis=1)
        product_tile = transposed_product(rows_in, stacked(refs[count:-2])).astype(jnp.bfloat16)

        @pl.when(pl.program_id(0) < tiles)
        def _():
            refs[-2][...] = product_tile

        @pl.when(pl.program_id(0) >= tiles)
        def _():
            refs[-1][...] = product_tile

    part = jax.ShapeDtypeStruct((part_rows, columns), jnp.bfloat16)
    return pl.pallas_call(
        body,
        out_shape=(part, part),
        grid=(2 * tiles,),
        in_specs=[pl.BlockSpec((tile, strip_depth), lambda at: (at, 0))] * count
        + [
            pl.BlockSpec(
                (block.shape[0], count * strip_depth),
                lambda at: (0, first),
                pipeline_mode=pl.Buffered(1),
            )
            for block in weight_blocks
        ],
        out_specs=(
            pl.BlockSpec((tile, columns), lambda at: (jnp.minimum(at, tiles - 1), 0)),
            pl.BlockSpec((tile, columns), lambda at: (jnp.maximum(at - tiles, 0), 0)),
        ),
        compiler_params=pltpu.CompilerParams(vmem_limit_bytes=VMEM_LIMIT),
        cost_estimate=pl.CostEstimate(
            flops=2 * rows * count * strip_depth * columns,
            bytes_accessed=2 * (rows * columns + count * strip_depth * (rows + columns)),
            transcendentals=0,
        ),
    )(*depth_parts, *weight_blocks)


def hidden_rows(mine, theirs, gate_blocks, lift_blocks, taps, bias, swapped, share, shares):
    part_rows, depth = mine.shape
    columns = gate_blocks[0].shape[1] // shares
    count = len(gate_blocks)
    width = next(width for width in (512, 384, 256, 128) if columns % width == 0)
    first_strip = share * (columns // width)

    chunk = 128

    def body(swapped_ref, mine_ref, theirs_ref, *refs):
        taps_ref, bias_ref, hidden_ref = refs[2 * count :]
        gate_weight, lift_weight = stacked(refs[:count]), stacked(refs[count : 2 * count])

        def rounded(rows_in, weight):
            wide = jnp.dot(rows_in, weight, preferred_element_type=jnp.float32)
            return wide.astype(jnp.bfloat16).astype(jnp.float32)

        def hidden_of(before, pre, lifted):
            padded = jnp.concatenate([before, pre], axis=0)
            filtered = bias_ref[...]
            for offset in range(TAPS):
                start = 8 - (TAPS - 1) + offset
                filtered = filtered + padded[start : start + pre.shape[0]] * taps_ref[offset : offset + 1, :]
            return (filtered * jax.nn.sigmoid(filtered) * lifted).astype(jnp.bfloat16)

        before = jnp.zeros((8, width), jnp.float32)
        for at, ref in enumerate((mine_ref, theirs_ref)):
            if at == 1:
                before = jnp.where(swapped_ref[0] == 0, before, 0.0)
            for first in range(0, part_rows, chunk):
                rows_in = ref[pl.ds(first, chunk), :]
                pre = rounded(rows_in, gate_weight)
                lifted = rounded(rows_in, lift_weight)
                hidden_ref[pl.ds(at * part_rows + first, chunk), :] = hidden_of(before, pre, lifted)
                before = pre[chunk - 8 :]
                if at == 0 and first == 0:
                    opening = pre[:16], lifted[:16]
        before = jnp.where(swapped_ref[0] == 1, before, 0.0)
        hidden_ref[pl.ds(0, 16), :] = hidden_of(before, *opening)

    def strip_at(rows, ahead=first_strip):
        return pl.BlockSpec((rows, width), lambda at, *_: (0, at + ahead))

    rows_spec = pl.BlockSpec(
        (part_rows, depth), lambda at, *_: (0, 0), pipeline_mode=pl.Buffered(1)
    )
    return pl.pallas_call(
        body,
        out_shape=jax.ShapeDtypeStruct((2 * part_rows, columns), jnp.bfloat16),
        grid_spec=pltpu.PrefetchScalarGridSpec(
            num_scalar_prefetch=1,
            grid=(columns // width,),
            in_specs=[rows_spec, rows_spec]
            + [strip_at(block.shape[0]) for block in gate_blocks + lift_blocks]
            + [strip_at(TAPS), strip_at(1)],
            out_specs=strip_at(2 * part_rows, 0),
        ),
        compiler_params=pltpu.CompilerParams(vmem_limit_bytes=VMEM_LIMIT),
        cost_estimate=pl.CostEstimate(
            flops=8 * part_rows * depth * columns,
            bytes_accessed=4 * (part_rows * (depth + columns) + depth * columns),
            transcendentals=2 * part_rows * columns,
        ),
    )(swapped, mine, theirs, *gate_blocks, *lift_blocks, taps, bias)


def by_row_tiles(body, owners, arrays, wide, outputs, tile=128):
    rows = arrays[0].shape[0]

    def tiled(array):
        return pl.BlockSpec((tile, array.shape[1]), lambda at, *_: (at, 0))

    return pl.pallas_call(
        body,
        out_shape=outputs,
        grid_spec=pltpu.PrefetchScalarGridSpec(
            num_scalar_prefetch=1,
            grid=(rows // tile,),
            in_specs=[tiled(array) for array in arrays]
            + [pl.BlockSpec(array.shape, lambda at, *_: (0, 0)) for array in wide],
            out_specs=[tiled(array) for array in outputs],
        ),
        compiler_params=pltpu.CompilerParams(vmem_limit_bytes=VMEM_LIMIT),
        cost_estimate=pl.CostEstimate(
            flops=200 * rows * arrays[0].shape[1],
            bytes_accessed=4 * rows * arrays[0].shape[1] * (len(arrays) + len(outputs)) // 2,
            transcendentals=rows,
        ),
    )(owners, *arrays, *wide)


def block_of(owners_ref, distance, width):
    return pl.ds(pl.multiple_of(owners_ref[distance] * width, width), width)


def norm_input(tokens, gain, owners, count):
    rows, features = tokens.shape
    width = features // count

    def body(owners_ref, tokens_ref, gain_ref, normed_ref):
        wide = tokens_ref[...].astype(jnp.float32)
        factor = lax.rsqrt(jnp.mean(wide * wide, axis=-1, keepdims=True) + norm_eps)
        for at in range(count):
            taken = block_of(owners_ref, at, width)
            normed_ref[:, at * width : (at + 1) * width] = (
                tokens_ref[:, taken].astype(jnp.float32) * factor * gain_ref[:, taken]
            ).astype(jnp.bfloat16)

    outputs = [jax.ShapeDtypeStruct((rows, features), jnp.bfloat16)]
    return by_row_tiles(body, owners, [tokens], [gain[None, :]], outputs)[0]


def norm_middle(tokens, parts, gain, owners, count):
    rows, features = tokens.shape
    width = features // count

    def body(owners_ref, tokens_ref, mine_ref, theirs_ref, far_ref, gain_ref, middle_ref, normed_ref):
        squares = jnp.zeros((tokens_ref.shape[0], 1), jnp.float32)
        for at in range(count):
            placed = slice(at * width, (at + 1) * width)
            taken = block_of(owners_ref, at, width)
            mixer = mine_ref[:, placed].astype(jnp.float32) + theirs_ref[:, placed].astype(jnp.float32)
            mixer = mixer + far_ref[:, placed].astype(jnp.float32)
            middle = tokens_ref[:, taken].astype(jnp.float32) + mixer
            middle_ref[:, placed] = middle
            squares = squares + jnp.sum(middle * middle, axis=-1, keepdims=True)
        factor = lax.rsqrt(squares / features + norm_eps)
        for at in range(count):
            placed = slice(at * width, (at + 1) * width)
            taken = block_of(owners_ref, at, width)
            normed_ref[:, placed] = (middle_ref[:, placed] * factor * gain_ref[:, taken]).astype(
                jnp.bfloat16
            )

    outputs = [
        jax.ShapeDtypeStruct((rows, features), jnp.float32),
        jax.ShapeDtypeStruct((rows, features), jnp.bfloat16),
    ]
    return by_row_tiles(body, owners, [tokens] + parts, [gain[None, :]], outputs)


def outcome_rows(middle, group_parts, groups, owners, count):
    rows, features = middle.shape
    width = features // count
    parts = [part for group in group_parts for part in group]

    def body(owners_ref, middle_ref, *refs):
        for number, group in enumerate(groups):
            mine_ref, theirs_ref, far_ref = refs[3 * number : 3 * number + 3]
            for order, at in enumerate(group):
                placed = slice(order * width, (order + 1) * width)
                channel = mine_ref[:, placed].astype(jnp.float32) + theirs_ref[:, placed].astype(jnp.float32)
                channel = channel + far_ref[:, placed].astype(jnp.float32)
                refs[-1][:, block_of(owners_ref, at, width)] = (
                    middle_ref[:, at * width : (at + 1) * width] + channel
                ).astype(jnp.bfloat16)

    outputs = [jax.ShapeDtypeStruct((rows, features), jnp.bfloat16)]
    return by_row_tiles(body, owners, [middle] + parts, [], outputs)[0]


def shards(
    tokens,
    mix_gain,
    query_weight,
    key_weight,
    value_weight,
    gate_weight,
    out_weight,
    head_gain,
    channel_gain,
    inner_gate,
    inner_lift,
    inner_down,
    filter_taps,
    filter_bias,
):
    tp_index = lax.axis_index("tp")
    rep_index = lax.axis_index("rep")
    fs_index = lax.axis_index("fs")
    count = lax.axis_size("fs")
    odd = fs_index % 2
    place = jnp.where(odd == 0, fs_index // 2, count - 1 - fs_index // 2)
    rows_dev, _ = tokens.shape
    length = rows_dev * 2
    cols = query_weight.shape[1] // 2
    hidden_cols = inner_gate.shape[1] // 2
    heads = cols // HEAD_DIM
    every = list(range(count))
    around = (place + jnp.arange(count, dtype=jnp.int32)) % count
    owners = jnp.where(around < count // 2, 2 * around, 2 * (count - around) - 1).astype(jnp.int32)
    swapped = tp_index.reshape(1).astype(jnp.int32)

    def part(weight, columns):
        return lax.dynamic_slice_in_dim(weight, rep_index * columns, columns, weight.ndim - 1)

    def joint(pieces):
        return jnp.concatenate(pieces, axis=-1)

    ring_a = Ring(joint([part(query_weight, cols), part(key_weight, cols)]), count, FAR_WAY["ra"])
    ring_b = Ring(
        joint([part(value_weight, cols), part(gate_weight, cols), part(out_weight, cols)]),
        count,
        FAR_WAY["rb"],
    )

    ring_g = Ring(after(part(inner_gate, hidden_cols), *ring_a.hops[-1]), count, FAR_WAY["rg"])
    ring_l = Ring(after(part(inner_lift, hidden_cols), *ring_b.hops[-1]), count, FAR_WAY["rl"])
    down = part(inner_down, hidden_cols)
    down_half = down.shape[0] // 2
    ring_c = Ring(after(down[:down_half], *ring_g.hops[-1]), count, FAR_WAY["rc"])
    ring_d = Ring(after(down[down_half:], *ring_l.hops[-1]), count, FAR_WAY["rd"])

    normed = norm_input(tokens, mix_gain, owners, count)
    far = swap(normed, "rep")
    own_in = [normed, swap(normed, "tp")]
    other_in = [far, swap(far, "tp")]

    positions = jnp.arange(length, dtype=jnp.float32)
    inverse = rope_base ** (
        -jnp.arange(HEAD_DIM // 2, dtype=jnp.float32) / (HEAD_DIM // 2)
    )
    angles = positions[:, None] * inverse[None, :]
    first_head = (tp_index * 2 + rep_index) * heads
    head_ids = (first_head + jnp.arange(heads, dtype=jnp.int32)).astype(jnp.float32)
    log_gamma = jnp.log(1.0 - 2.0 ** (-5.0 - head_ids))
    gain_dev = lax.dynamic_slice_in_dim(head_gain, first_head * HEAD_DIM, cols, 0)
    tables = (jnp.cos(angles), jnp.sin(angles), gain_dev, log_gamma, swapped)
    early_blocks, late_blocks = ring_a.parts(every), ring_b.parts(every)

    def mixer_part(rows_in):
        query_key = project_rows(rows_in, early_blocks, 2 * cols)
        value_gate = project_rows(rows_in, late_blocks, 2 * cols)
        mixed = mix_heads(query_key, value_gate, *tables)
        return project_back([mixed], late_blocks, 2)

    other_mine, other_theirs = mixer_part(other_in)
    other_sum = other_mine.astype(jnp.float32) + swap(other_theirs, "tp").astype(jnp.float32)
    far = swap(other_sum.astype(jnp.bfloat16), "rep")
    own_mine, own_theirs = mixer_part(own_in)
    middle, normed_mid = norm_middle(
        tokens, [own_mine, swap(own_theirs, "tp"), far], channel_gain, owners, count
    )
    far = swap(normed_mid, "rep")
    own_mid = [normed_mid, swap(normed_mid, "tp")]
    other_mid = [far, swap(far, "tp")]

    first_hidden = (tp_index * 2 + rep_index) * hidden_cols

    taps = lax.dynamic_slice_in_dim(filter_taps, first_hidden, hidden_cols, 1)
    bias = lax.dynamic_slice_in_dim(filter_bias, first_hidden, hidden_cols, 0)[None, :]
    hidden_blocks = ring_g.parts(every), ring_l.parts(every)

    def hidden_strips(rows_in, shares):
        return [
            hidden_rows(*rows_in, *hidden_blocks, taps, bias, swapped, share, shares)
            for share in range(shares)
        ]

    own_hidden = hidden_strips(own_mid, 2)
    other_hidden = hidden_strips(other_mid, 1)
    near = count // 2 - 2
    groups = [
        [at for at in every if min(at, count - at) <= near],
        [at for at in every if min(at, count - at) > near],
    ]
    group_parts = []
    for group in groups:
        blocks = [
            piece for at in group for ring in (ring_c, ring_d) for piece in ring.parts([at])
        ]
        other_mine, other_theirs = project_back(other_hidden, blocks)
        theirs = swap(other_theirs, "tp")
        other_sum = other_mine.astype(jnp.float32) + theirs.astype(jnp.float32)
        far = swap(other_sum.astype(jnp.bfloat16), "rep")
        own_mine, own_theirs = project_back(own_hidden, blocks)
        group_parts.append([own_mine, swap(own_theirs, "tp"), far])
    return outcome_rows(middle, group_parts, groups, owners, count)


def split_pays(mesh):
    sizes = mesh.shape
    return sizes["rep"] == 2 and sizes["tp"] == 2 and sizes["fs"] % 2 == 0 and sizes["fs"] >= 8


def solution(mesh):
    in_specs = (
        P(("rep", "fs", "tp"), None),
        P(),
        P("fs", "tp"),
        P("fs", "tp"),
        P("fs", "tp"),
        P("fs", "tp"),
        P("fs", "tp"),
        P(),
        P(),
        P("fs", "tp"),
        P("fs", "tp"),
        P("fs", "tp"),
        P(),
        P(),
    )
    out_specs = P(("rep", "fs", "tp"), None)
    if not split_pays(mesh):
        return jax.shard_map(
            shards_any, mesh=mesh, in_specs=in_specs, out_specs=out_specs, check_vma=False
        )
    return jax.shard_map(shards, mesh=mesh, in_specs=in_specs, out_specs=out_specs, check_vma=False)
```

profile of v0, /device:TPU:0, one launch (start us, length us, event | category | flops | bytes accessed | tf_op | source)
XLA Modules:
  0.0 523.8 jit_solution(15197804295837994641)
XLA Ops:
  11.3 43.0 %collective-permute-done.16.refs_0_ = bf16[512,2048]{1,0:T(8,128)(2,1)} collective-permute-done((bf16[512,2048]{1,0:T(8,128)(2,1)}, bf16[512,2048]{1,0:T(8,128)(2,1)}, u32[]{:S(2)}, u32[]{:S(2)}) %collective-permute-start.16) | collective-permute-done | bytes 2097184 | tf_op jit(solution)/shard_map/ppermute | solution.py:318
  59.2 15.5 %collective-permute-done.12.refs_9_.refs_8_ = bf16[256,1536]{1,0:T(8,128)(2,1)S(1)} collective-permute-done((bf16[256,1536]{1,0:T(8,128)(2,1)S(1)}, bf16[256,1536]{1,0:T(8,128)(2,1)S(1)}, u32[]{:S(2)}, u32[]{:S(2)}) %collective-permute-start.12) | collective-permute-done | bytes 786464 | tf_op jit(solution)/shard_map/ppermute | solution.py:297
  78.5 9.3 %collective-permute-done.1.refs_3_ = bf16[256,1024]{1,0:T(8,128)(2,1)S(1)} collective-permute-done((bf16[256,1024]{1,0:T(8,128)(2,1)S(1)}, bf16[256,1024]{1,0:T(8,128)(2,1)S(1)}, u32[]{:S(2)}, u32[]{:S(2)}) %collective-permute-start.1) | collective-permute-done | bytes 524320 | tf_op jit(solution)/shard_map/ppermute | solution.py:301
  91.3 23.9 %collective-permute-done.2.refs_4_ = bf16[256,1024]{1,0:T(8,128)(2,1)} collective-permute-done((bf16[256,1024]{1,0:T(8,128)(2,1)S(1)}, bf16[256,1024]{1,0:T(8,128)(2,1)}, u32[]{:S(2)}, u32[]{:S(2)}) %collective-permute-start.2) | collective-permute-done | bytes 524320 | tf_op jit(solution)/shard_map/ppermute | solution.py:301
  122.0 8.3 %collective-permute-done.3.refs_5_ = bf16[256,1024]{1,0:T(8,128)(2,1)} collective-permute-done((bf16[256,1024]{1,0:T(8,128)(2,1)}, bf16[256,1024]{1,0:T(8,128)(2,1)}, u32[]{:S(2)}, u32[]{:S(2)}) %collective-permute-start.3) | collective-permute-done | bytes 524320 | tf_op jit(solution)/shard_map/ppermute | solution.py:301
  132.7 8.5 %shard_map.141.query_ref.key_ref = bf16[1024,1024]{1,0:T(8,128)(2,1)S(1)} custom-call(bf16[512,2048]{1,0:T(8,128)(2,1)} %collective-permute-done.16.refs_0_, bf16[512,2048]{1,0:T(8,128)(2,1)} %collective-permute-done.17.refs_1_, bf16[256,1024]{1,0:T(8,128)(2,1)S(1)} %pad_maximum_fusion.1.refs_2_, bf16[256,1024]{1,0:T(8,128)(2,1)S(1)} %copy-done.34, ...), custom_call_target="tpu_custom_call" | custom-call | flops 4294967296 | bytes 10485760 | tf_op jit(solution)/shard_map/pallas_call | solution.py:447
  141.2 4.5 collective-permute-done.14.refs_7_.refs_6_
  145.7 8.0 %shard_map.142.value_ref.gate_ref = bf16[1024,1024]{1,0:T(8,128)(2,1)S(1)} custom-call(bf16[512,2048]{1,0:T(8,128)(2,1)} %collective-permute-done.16.refs_0_, bf16[512,2048]{1,0:T(8,128)(2,1)} %collective-permute-done.17.refs_1_, bf16[256,1536]{1,0:T(8,128)(2,1)S(1)} %pad_maximum_fusion.refs_2_.refs_1_, bf16[256,1536]{1,0:T(8,128)(2,1)S(1)} %copy-done.28, ...), custom_call_target="tpu_custom_call" | custom-call | flops 4294967296 | bytes 10485760 | tf_op jit(solution)/shard_map/pallas_call | solution.py:447
  153.7 5.1 shard_map.143.refs_0_
  158.8 4.8 shard_map.144
  163.7 7.4 %shard_map.137.query_ref.key_ref = bf16[1024,1024]{1,0:T(8,128)(2,1)S(1)} custom-call(bf16[512,2048]{1,0:T(8,128)(2,1)} %shard_map.136.refs_0_, bf16[512,2048]{1,0:T(8,128)(2,1)S(1)} %collective-permute-done.refs_1_, bf16[256,1024]{1,0:T(8,128)(2,1)S(1)} %pad_maximum_fusion.1.refs_2_, bf16[256,1024]{1,0:T(8,128)(2,1)S(1)} %copy-done.35, ...), custom_call_target="tpu_custom_call" | custom-call | flops 4294967296 | bytes 10485760 | tf_op jit(solution)/shard_map/pallas_call | solution.py:447
  171.1 7.3 %shard_map.138.value_ref.gate_ref = bf16[1024,1024]{1,0:T(8,128)(2,1)S(1)} custom-call(bf16[512,2048]{1,0:T(8,128)(2,1)} %shard_map.136.refs_0_, bf16[512,2048]{1,0:T(8,128)(2,1)S(1)} %collective-permute-done.refs_1_, bf16[256,1536]{1,0:T(8,128)(2,1)S(1)} %pad_maximum_fusion.refs_2_.refs_1_, bf16[256,1536]{1,0:T(8,128)(2,1)S(1)} %copy-done.28, ...), custom_call_target="tpu_custom_call" | custom-call | flops 4294967296 | bytes 10485760 | tf_op jit(solution)/shard_map/pallas_call | solution.py:447
  178.5 5.1 shard_map.139.refs_0_
  183.6 5.8 %shard_map.140 = (bf16[512,2048]{1,0:T(8,128)(2,1)S(1)}, bf16[512,2048]{1,0:T(8,128)(2,1)}) custom-call(bf16[1024,512]{1,0:T(8,128)(2,1)S(1)} %shard_map.139.refs_0_, bf16[256,1536]{1,0:T(8,128)(2,1)S(1)} %pad_maximum_fusion.refs_2_.refs_1_, bf16[256,1536]{1,0:T(8,128)(2,1)S(1)} %copy-done.28, bf16[256,1536]{1,0:T(8,128)(2,1)S(1)} %copy-done.32, ...), custom_call_target="tpu_custom_call" | custom-call | flops 2147483648 | bytes 7340032 | tf_op jit(solution)/shard_map/pallas_call | solution.py:484
  197.1 42.9 %collective-permute-done.19.far_ref = bf16[512,2048]{1,0:T(8,128)(2,1)} collective-permute-done((bf16[512,2048]{1,0:T(8,128)(2,1)}, bf16[512,2048]{1,0:T(8,128)(2,1)}, u32[]{:S(2)}, u32[]{:S(2)}) %collective-permute-start.19) | collective-permute-done | bytes 2097184 | tf_op jit(solution)/shard_map/ppermute | solution.py:318
  254.6 15.5 %collective-permute-done.25.refs_6_ = bf16[256,1536]{1,0:T(8,128)(2,1)S(1)} collective-permute-done((bf16[256,1536]{1,0:T(8,128)(2,1)S(1)}, bf16[256,1536]{1,0:T(8,128)(2,1)S(1)}, u32[]{:S(2)}, u32[]{:S(2)}) %collective-permute-start.25) | collective-permute-done | bytes 786464 | tf_op jit(solution)/shard_map/ppermute | solution.py:297
  273.9 14.6 %collective-permute-done.21.refs_1_ = bf16[256,1536]{1,0:T(8,128)(2,1)S(1)} collective-permute-done((bf16[256,1536]{1,0:T(8,128)(2,1)S(1)}, bf16[256,1536]{1,0:T(8,128)(2,1)S(1)}, u32[]{:S(2)}, u32[]{:S(2)}) %collective-permute-start.21) | collective-permute-done | bytes 786464 | tf_op jit(solution)/shard_map/ppermute | solution.py:301
  294.9 9.0 %collective-permute-done.26.refs_5_ = bf16[256,1536]{1,0:T(8,128)(2,1)} collective-permute-done((bf16[256,1536]{1,0:T(8,128)(2,1)S(1)}, bf16[256,1536]{1,0:T(8,128)(2,1)}, u32[]{:S(2)}, u32[]{:S(2)}) %collective-permute-start.26) | collective-permute-done | bytes 786464 | tf_op jit(solution)/shard_map/ppermute | solution.py:297
  305.9 16.4 %collective-permute-done.22.refs_2_ = bf16[256,1536]{1,0:T(8,128)(2,1)} collective-permute-done((bf16[256,1536]{1,0:T(8,128)(2,1)S(1)}, bf16[256,1536]{1,0:T(8,128)(2,1)}, u32[]{:S(2)}, u32[]{:S(2)}) %collective-permute-start.22) | collective-permute-done | bytes 786464 | tf_op jit(solution)/shard_map/ppermute | solution.py:301
  325.5 12.1 %collective-permute-done.27.refs_4_ = bf16[256,1536]{1,0:T(8,128)(2,1)} collective-permute-done((bf16[256,1536]{1,0:T(8,128)(2,1)}, bf16[256,1536]{1,0:T(8,128)(2,1)}, u32[]{:S(2)}, u32[]{:S(2)}) %collective-permute-start.27) | collective-permute-done | bytes 786464 | tf_op jit(solution)/shard_map/ppermute | solution.py:297
  340.7 15.3 %collective-permute-done.23.refs_3_ = bf16[256,1536]{1,0:T(8,128)(2,1)} collective-permute-done((bf16[256,1536]{1,0:T(8,128)(2,1)}, bf16[256,1536]{1,0:T(8,128)(2,1)}, u32[]{:S(2)}, u32[]{:S(2)}) %collective-permute-start.23) | collective-permute-done | bytes 786464 | tf_op jit(solution)/shard_map/ppermute | solution.py:301
  356.4 7.8 %collective-permute-done.35.refs_4_.refs_3_ = bf16[128,1536]{1,0:T(8,128)(2,1)S(1)} collective-permute-done((bf16[128,1536]{1,0:T(8,128)(2,1)S(1)}, bf16[128,1536]{1,0:T(8,128)(2,1)S(1)}, u32[]{:S(2)}, u32[]{:S(2)}) %collective-permute-start.35) | collective-permute-done | bytes 393248 | tf_op jit(solution)/shard_map/ppermute | solution.py:301
  374.0 7.2 %collective-permute-done.37.refs_6_.refs_5_ = bf16[128,1536]{1,0:T(8,128)(2,1)S(1)} collective-permute-done((bf16[128,1536]{1,0:T(8,128)(2,1)S(1)}, bf16[128,1536]{1,0:T(8,128)(2,1)S(1)}, u32[]{:S(2)}, u32[]{:S(2)}) %collective-permute-start.37) | collective-permute-done | bytes 393248 | tf_op jit(solution)/shard_map/ppermute | solution.py:301
  394.0 7.4 %collective-permute-done.42.refs_9_.refs_8_ = bf16[128,1536]{1,0:T(8,128)(2,1)} collective-permute-done((bf16[128,1536]{1,0:T(8,128)(2,1)}, bf16[128,1536]{1,0:T(8,128)(2,1)}, u32[]{:S(2)}, u32[]{:S(2)}) %collective-permute-start.42) | collective-permute-done | bytes 393248 | tf_op jit(solution)/shard_map/ppermute | solution.py:297
  410.9 18.2 %shard_map.149.refs_0_ = bf16[1024,1536]{1,0:T(8,128)(2,1)S(1)} custom-call(s32[1]{0:T(128)} %bitcast.swapped_ref, bf16[512,2048]{1,0:T(8,128)(2,1)} %collective-permute-done.44.mine_ref, bf16[512,2048]{1,0:T(8,128)(2,1)} %collective-permute-done.45.theirs_ref, bf16[256,1536]{1,0:T(8,128)(2,1)S(1)} %constant_dynamic-slice_fusion.3.refs_0_, ...), custom_call_target="tpu_custom_call" | custom-call | flops 12884901888 | bytes 19922944 | tf_op jit(solution)/shard_map/pallas_call | solution.py:556
  429.2 6.7 %shard_map.150 = (bf16[512,1280]{1,0:T(8,128)(2,1)S(1)}, bf16[512,1280]{1,0:T(8,128)(2,1)S(1)}) custom-call(bf16[1024,1536]{1,0:T(8,128)(2,1)S(1)} %shard_map.149.refs_0_, bf16[128,1536]{1,0:T(8,128)(2,1)S(1)} %get-tuple-element.31.refs_2_.refs_1_, bf16[128,1536]{1,0:T(8,128)(2,1)S(1)} %get-tuple-element.32.refs_3_.refs_2_, ...), custom_call_target="tpu_custom_call" | custom-call | flops 4026531840 | bytes 9699328 | tf_op jit(solution)/shard_map/pallas_call | solution.py:484
  436.0 12.2 %shard_map.146.refs_0_ = bf16[1024,768]{1,0:T(8,128)(2,1)S(1)} custom-call(s32[1]{0:T(128)} %bitcast.swapped_ref, bf16[512,2048]{1,0:T(8,128)(2,1)S(1)} %copy-done.11, bf16[512,2048]{1,0:T(8,128)(2,1)} %collective-permute-done.20.theirs_ref, bf16[256,1536]{1,0:T(8,128)(2,1)S(1)} %constant_dynamic-slice_fusion.3.refs_0_, bf16[256,1536]{1,0:T(8,128)(2,1)S(1)} %copy-done.23, ...), custom_call_target="tpu_custom_call" | custom-call | flops 6442450944 | bytes 12058624 | tf_op jit(solution)/shard_map/pallas_call | solution.py:556
  448.2 12.4 %shard_map.147.refs_1_ = bf16[1024,768]{1,0:T(8,128)(2,1)S(1)} custom-call(s32[1]{0:T(128)} %bitcast.swapped_ref, bf16[512,2048]{1,0:T(8,128)(2,1)S(1)} %copy-done.11, bf16[512,2048]{1,0:T(8,128)(2,1)} %collective-permute-done.20.theirs_ref, bf16[256,1536]{1,0:T(8,128)(2,1)S(1)} %constant_dynamic-slice_fusion.3.refs_0_, bf16[256,1536]{1,0:T(8,128)(2,1)S(1)} %copy-done.23, ...), custom_call_target="tpu_custom_call" | custom-call | flops 6442450944 | bytes 12058624 | tf_op jit(solution)/shard_map/pallas_call | solution.py:556
  460.6 6.5 %shard_map.148 = (bf16[512,1280]{1,0:T(8,128)(2,1)S(1)}, bf16[512,1280]{1,0:T(8,128)(2,1)S(1)}) custom-call(bf16[1024,768]{1,0:T(8,128)(2,1)S(1)} %shard_map.146.refs_0_, bf16[1024,768]{1,0:T(8,128)(2,1)S(1)} %shard_map.147.refs_1_, bf16[128,1536]{1,0:T(8,128)(2,1)S(1)} %get-tuple-element.31.refs_2_.refs_1_, ...), custom_call_target="tpu_custom_call" | custom-call | flops 4026531840 | bytes 9699328 | tf_op jit(solution)/shard_map/pallas_call | solution.py:484
  467.7 4.5 shard_map.152
  473.2 4.7 shard_map.151
  480.3 40.4 %collective-permute-done.56.refs_5_ = bf16[512,768]{1,0:T(8,128)(2,1)S(1)} collective-permute-done((bf16[512,768]{1,0:T(8,128)(2,1)S(1)}, bf16[512,768]{1,0:T(8,128)(2,1)S(1)}, u32[]{:S(2)}, u32[]{:S(2)}) %collective-permute-start.56) | collective-permute-done | bytes 786464 | tf_op jit(solution)/shard_map/ppermute | solution.py:318
  (219 shorter events, 113.0 us)
Async XLA Ops:
  5.4 48.9 %collective-permute-start.16 = (bf16[512,2048]{1,0:T(8,128)(2,1)}, bf16[512,2048]{1,0:T(8,128)(2,1)}, u32[]{:S(2)}, u32[]{:S(2)}) collective-permute-start(bf16[512,2048]{1,0:T(8,128)(2,1)} %shard_map.136.refs_0_), channel_id=1, source_target_pairs={{0,16},{16,0},{1,17},{17,1},{2,18},{18,2},{3,19},{19,3},{4,20},{20... | collective-permute-start | bytes 6291464 | tf_op jit(solution)/shard_map/ppermute | solution.py:318
  8.5 47.6 %collective-permute-start.8 = (bf16[256,1536]{1,0:T(8,128)(2,1)S(1)}, bf16[256,1536]{1,0:T(8,128)(2,1)S(1)}, u32[]{:S(2)}, u32[]{:S(2)}) collective-permute-start(bf16[256,1536]{1,0:T(8,128)(2,1)S(1)} %pad_maximum_fusion.refs_2_.refs_1_), channel_id=1, source_target_pairs={{4,0},{8,4},{12,8},{14,12},{10,14},{6,10},{2,6},{0,2},{5,1},{9,5},... | collective-permute-start | bytes 2359304 | tf_op jit(solution)/shard_map/ppermute | solution.py:301
  10.2 48.8 %collective-permute-start.4 = (bf16[256,1024]{1,0:T(8,128)(2,1)S(1)}, bf16[256,1024]{1,0:T(8,128)(2,1)S(1)}, u32[]{:S(2)}, u32[]{:S(2)}) collective-permute-start(bf16[256,1024]{1,0:T(8,128)(2,1)S(1)} %pad_maximum_fusion.1.refs_2_), channel_id=1, source_target_pairs={{0,4},{4,8},{8,12},{12,14},{14,10},{10,6},{6,2},{2,0},{1,5},{5,9},... | collective-permute-start | bytes 1572872 | tf_op jit(solution)/shard_map/ppermute | solution.py:297
  54.3 76.3 %collective-permute-start.17 = (bf16[512,2048]{1,0:T(8,128)(2,1)}, bf16[512,2048]{1,0:T(8,128)(2,1)}, u32[]{:S(2)}, u32[]{:S(2)}) collective-permute-start(bf16[512,2048]{1,0:T(8,128)(2,1)} %collective-permute-done.16.refs_0_), channel_id=1, source_target_pairs={{0,1},{1,0},{2,3},{3,2},{4,5},{5,4},{6,7},{7,6},{8,9},{9,8},{10,11... | collective-permute-start | bytes 6291464 | tf_op jit(solution)/shard_map/ppermute | solution.py:318
  57.2 30.6 %collective-permute-start.1 = (bf16[256,1024]{1,0:T(8,128)(2,1)S(1)}, bf16[256,1024]{1,0:T(8,128)(2,1)S(1)}, u32[]{:S(2)}, u32[]{:S(2)}) collective-permute-start(bf16[256,1024]{1,0:T(8,128)(2,1)S(1)} %pad_maximum_fusion.1.refs_2_), channel_id=1, source_target_pairs={{4,0},{8,4},{12,8},{14,12},{10,14},{6,10},{2,6},{0,2},{5,1},{9,5},... | collective-permute-start | bytes 1572872 | tf_op jit(solution)/shard_map/ppermute | solution.py:301
  59.0 29.8 %collective-permute-start.5 = (bf16[256,1024]{1,0:T(8,128)(2,1)S(1)}, bf16[256,1024]{1,0:T(8,128)(2,1)S(1)}, u32[]{:S(2)}, u32[]{:S(2)}) collective-permute-start(bf16[256,1024]{1,0:T(8,128)(2,1)S(1)} %collective-permute-done.4.refs_9_), channel_id=1, source_target_pairs={{0,4},{4,8},{8,12},{12,14},{14,10},{10,6},{6,2},{2,0},{1,5},{5,9},... | collective-permute-start | bytes 1572872 | tf_op jit(solution)/shard_map/ppermute | solution.py:297
  74.7 42.6 %collective-permute-start.13 = (bf16[256,1536]{1,0:T(8,128)(2,1)S(1)}, bf16[256,1536]{1,0:T(8,128)(2,1)}, u32[]{:S(2)}, u32[]{:S(2)}) collective-permute-start(bf16[256,1536]{1,0:T(8,128)(2,1)S(1)} %collective-permute-done.12.refs_9_.refs_8_), channel_id=1, source_target_pairs={{0,4},{4,8},{8,12},{12,14},{14,10},{10,6},{6,2},{2,0},{1,5},{5,9},... | collective-permute-start | bytes 2359304 | tf_op jit(solution)/shard_map/ppermute | solution.py:297
  77.4 41.4 %collective-permute-start.10 = (bf16[256,1536]{1,0:T(8,128)(2,1)S(1)}, bf16[256,1536]{1,0:T(8,128)(2,1)}, u32[]{:S(2)}, u32[]{:S(2)}) collective-permute-start(bf16[256,1536]{1,0:T(8,128)(2,1)S(1)} %collective-permute-done.9.refs_4_.refs_3_), channel_id=1, source_target_pairs={{4,0},{8,4},{12,8},{14,12},{10,14},{6,10},{2,6},{0,2},{5,1},{9,5},... | collective-permute-start | bytes 2359304 | tf_op jit(solution)/shard_map/ppermute | solution.py:301
  130.3 33.4 %collective-permute-start = (bf16[512,2048]{1,0:T(8,128)(2,1)}, bf16[512,2048]{1,0:T(8,128)(2,1)S(1)}, u32[]{:S(2)}, u32[]{:S(2)}) collective-permute-start(bf16[512,2048]{1,0:T(8,128)(2,1)} %shard_map.136.refs_0_), channel_id=1, source_target_pairs={{0,1},{1,0},{2,3},{3,2},{4,5},{5,4},{6,7},{7,6},{8,9},{9,8},{10,11... | collective-permute-start | bytes 6291464 | tf_op jit(solution)/shard_map/ppermute | solution.py:318
  192.1 47.9 %collective-permute-start.19 = (bf16[512,2048]{1,0:T(8,128)(2,1)}, bf16[512,2048]{1,0:T(8,128)(2,1)}, u32[]{:S(2)}, u32[]{:S(2)}) collective-permute-start(bf16[512,2048]{1,0:T(8,128)(2,1)} %add_convert_fusion), channel_id=1, source_target_pairs={{0,16},{16,0},{1,17},{17,1},{2,18},{18,2},{3,19},{19,3},{4,20},{20... | collective-permute-start | bytes 6291464 | tf_op jit(solution)/shard_map/ppermute | solution.py:318
  193.7 55.9 %collective-permute-start.24 = (bf16[256,1536]{1,0:T(8,128)(2,1)S(1)}, bf16[256,1536]{1,0:T(8,128)(2,1)S(1)}, u32[]{:S(2)}, u32[]{:S(2)}) collective-permute-start(bf16[256,1536]{1,0:T(8,128)(2,1)S(1)} %constant_dynamic-slice_fusion.3.refs_0_), channel_id=1, source_target_pairs={{0,4},{4,8},{8,12},{12,14},{14,10},{10,6},{6,2},{2,0},{1,5},{5,9},... | collective-permute-start | bytes 2359304 | tf_op jit(solution)/shard_map/ppermute | solution.py:297
  196.5 54.7 %collective-permute-start.28 = (bf16[256,1536]{1,0:T(8,128)(2,1)S(1)}, bf16[256,1536]{1,0:T(8,128)(2,1)S(1)}, u32[]{:S(2)}, u32[]{:S(2)}) collective-permute-start(bf16[256,1536]{1,0:T(8,128)(2,1)S(1)} %constant_dynamic-slice_fusion.2.refs_8_), channel_id=1, source_target_pairs={{4,0},{8,4},{12,8},{14,12},{10,14},{6,10},{2,6},{0,2},{5,1},{9,5},... | collective-permute-start | bytes 2359304 | tf_op jit(solution)/shard_map/ppermute | solution.py:301
  248.0 46.8 %collective-permute-start.44 = (bf16[512,2048]{1,0:T(8,128)(2,1)S(1)}, bf16[512,2048]{1,0:T(8,128)(2,1)}, u32[]{:S(2)}, u32[]{:S(2)}) collective-permute-start(bf16[512,2048]{1,0:T(8,128)(2,1)S(1)} %get-tuple-element.28.mine_ref), channel_id=1, source_target_pairs={{0,16},{16,0},{1,17},{17,1},{2,18},{18,2},{3,19},{19,3},{4,20},{20... | collective-permute-start | bytes 6291464 | tf_op jit(solution)/shard_map/ppermute | solution.py:318
  252.5 35.9 %collective-permute-start.21 = (bf16[256,1536]{1,0:T(8,128)(2,1)S(1)}, bf16[256,1536]{1,0:T(8,128)(2,1)S(1)}, u32[]{:S(2)}, u32[]{:S(2)}) collective-permute-start(bf16[256,1536]{1,0:T(8,128)(2,1)S(1)} %constant_dynamic-slice_fusion.3.refs_0_), channel_id=1, source_target_pairs={{4,0},{8,4},{12,8},{14,12},{10,14},{6,10},{2,6},{0,2},{5,1},{9,5},... | collective-permute-start | bytes 2359304 | tf_op jit(solution)/shard_map/ppermute | solution.py:301
  254.0 35.8 %collective-permute-start.32 = (bf16[256,1536]{1,0:T(8,128)(2,1)S(1)}, bf16[256,1536]{1,0:T(8,128)(2,1)S(1)}, u32[]{:S(2)}, u32[]{:S(2)}) collective-permute-start(bf16[256,1536]{1,0:T(8,128)(2,1)S(1)} %constant_dynamic-slice_fusion.2.refs_8_), channel_id=1, source_target_pairs={{0,4},{4,8},{8,12},{12,14},{14,10},{10,6},{6,2},{2,0},{1,5},{5,9},... | collective-permute-start | bytes 2359304 | tf_op jit(solution)/shard_map/ppermute | solution.py:297
  270.0 33.8 %collective-permute-start.26 = (bf16[256,1536]{1,0:T(8,128)(2,1)S(1)}, bf16[256,1536]{1,0:T(8,128)(2,1)}, u32[]{:S(2)}, u32[]{:S(2)}) collective-permute-start(bf16[256,1536]{1,0:T(8,128)(2,1)S(1)} %collective-permute-done.25.refs_6_), channel_id=1, source_target_pairs={{0,4},{4,8},{8,12},{12,14},{14,10},{10,6},{6,2},{2,0},{1,5},{5,9},... | collective-permute-start | bytes 2359304 | tf_op jit(solution)/shard_map/ppermute | solution.py:297
  272.5 32.9 %collective-permute-start.30 = (bf16[256,1536]{1,0:T(8,128)(2,1)S(1)}, bf16[256,1536]{1,0:T(8,128)(2,1)}, u32[]{:S(2)}, u32[]{:S(2)}) collective-permute-start(bf16[256,1536]{1,0:T(8,128)(2,1)S(1)} %collective-permute-done.29.refs_10_), channel_id=1, source_target_pairs={{4,0},{8,4},{12,8},{14,12},{10,14},{6,10},{2,6},{0,2},{5,1},{9,5},... | collective-permute-start | bytes 2359304 | tf_op jit(solution)/shard_map/ppermute | solution.py:301
  288.5 33.8 %collective-permute-start.22 = (bf16[256,1536]{1,0:T(8,128)(2,1)S(1)}, bf16[256,1536]{1,0:T(8,128)(2,1)}, u32[]{:S(2)}, u32[]{:S(2)}) collective-permute-start(bf16[256,1536]{1,0:T(8,128)(2,1)S(1)} %collective-permute-done.21.refs_1_), channel_id=1, source_target_pairs={{4,0},{8,4},{12,8},{14,12},{10,14},{6,10},{2,6},{0,2},{5,1},{9,5},... | collective-permute-start | bytes 2359304 | tf_op jit(solution)/shard_map/ppermute | solution.py:301
  289.8 32.9 %collective-permute-start.33 = (bf16[256,1536]{1,0:T(8,128)(2,1)S(1)}, bf16[256,1536]{1,0:T(8,128)(2,1)}, u32[]{:S(2)}, u32[]{:S(2)}) collective-permute-start(bf16[256,1536]{1,0:T(8,128)(2,1)S(1)} %collective-permute-done.32.refs_15_), channel_id=1, source_target_pairs={{0,4},{4,8},{8,12},{12,14},{14,10},{10,6},{6,2},{2,0},{1,5},{5,9},... | collective-permute-start | bytes 2359304 | tf_op jit(solution)/shard_map/ppermute | solution.py:297
  294.9 109.7 %collective-permute-start.45 = (bf16[512,2048]{1,0:T(8,128)(2,1)}, bf16[512,2048]{1,0:T(8,128)(2,1)}, u32[]{:S(2)}, u32[]{:S(2)}) collective-permute-start(bf16[512,2048]{1,0:T(8,128)(2,1)} %collective-permute-done.44.mine_ref), channel_id=1, source_target_pairs={{0,1},{1,0},{2,3},{3,2},{4,5},{5,4},{6,7},{7,6},{8,9},{9,8},{10,11... | collective-permute-start | bytes 6291464 | tf_op jit(solution)/shard_map/ppermute | solution.py:318
  303.9 33.7 %collective-permute-start.27 = (bf16[256,1536]{1,0:T(8,128)(2,1)}, bf16[256,1536]{1,0:T(8,128)(2,1)}, u32[]{:S(2)}, u32[]{:S(2)}) collective-permute-start(bf16[256,1536]{1,0:T(8,128)(2,1)} %collective-permute-done.26.refs_5_), channel_id=1, source_target_pairs={{0,4},{4,8},{8,12},{12,14},{14,10},{10,6},{6,2},{2,0},{1,5},{5,9},... | collective-permute-start | bytes 2359304 | tf_op jit(solution)/shard_map/ppermute | solution.py:297
  305.4 33.7 %collective-permute-start.31 = (bf16[256,1536]{1,0:T(8,128)(2,1)}, bf16[256,1536]{1,0:T(8,128)(2,1)}, u32[]{:S(2)}, u32[]{:S(2)}) collective-permute-start(bf16[256,1536]{1,0:T(8,128)(2,1)} %collective-permute-done.30.refs_11_), channel_id=1, source_target_pairs={{4,0},{8,4},{12,8},{14,12},{10,14},{6,10},{2,6},{0,2},{5,1},{9,5},... | collective-permute-start | bytes 2359304 | tf_op jit(solution)/shard_map/ppermute | solution.py:301
  322.3 33.7 %collective-permute-start.23 = (bf16[256,1536]{1,0:T(8,128)(2,1)}, bf16[256,1536]{1,0:T(8,128)(2,1)}, u32[]{:S(2)}, u32[]{:S(2)}) collective-permute-start(bf16[256,1536]{1,0:T(8,128)(2,1)} %collective-permute-done.22.refs_2_), channel_id=1, source_target_pairs={{4,0},{8,4},{12,8},{14,12},{10,14},{6,10},{2,6},{0,2},{5,1},{9,5},... | collective-permute-start | bytes 2359304 | tf_op jit(solution)/shard_map/ppermute | solution.py:301
  322.7 44.3 %collective-permute-start.34 = (bf16[256,1536]{1,0:T(8,128)(2,1)}, bf16[256,1536]{1,0:T(8,128)(2,1)}, u32[]{:S(2)}, u32[]{:S(2)}) collective-permute-start(bf16[256,1536]{1,0:T(8,128)(2,1)} %collective-permute-done.33.refs_14_), channel_id=1, source_target_pairs={{0,4},{4,8},{8,12},{12,14},{14,10},{10,6},{6,2},{2,0},{1,5},{5,9},... | collective-permute-start | bytes 2359304 | tf_op jit(solution)/shard_map/ppermute | solution.py:297
  381.1 54.7 %collective-permute-start.20 = (bf16[512,2048]{1,0:T(8,128)(2,1)}, bf16[512,2048]{1,0:T(8,128)(2,1)}, u32[]{:S(2)}, u32[]{:S(2)}) collective-permute-start(bf16[512,2048]{1,0:T(8,128)(2,1)} %copy-done.10), channel_id=1, source_target_pairs={{0,1},{1,0},{2,3},{3,2},{4,5},{5,4},{6,7},{7,6},{8,9},{9,8},{10,11... | collective-permute-start | bytes 6291464 | tf_op jit(solution)/shard_map/ppermute | solution.py:318
  393.5 73.6 %collective-permute-start.48 = (bf16[128,1536]{1,0:T(8,128)(2,1)}, bf16[128,1536]{1,0:T(8,128)(2,1)S(1)}, u32[]{:S(2)}, u32[]{:S(2)}) collective-permute-start(bf16[128,1536]{1,0:T(8,128)(2,1)} %copy-done.43), channel_id=1, source_target_pairs={{4,0},{8,4},{12,8},{14,12},{10,14},{6,10},{2,6},{0,2},{5,1},{9,5},... | collective-permute-start | bytes 1179656 | tf_op jit(solution)/shard_map/ppermute | solution.py:301
  401.4 66.2 %collective-permute-start.51 = (bf16[128,1536]{1,0:T(8,128)(2,1)}, bf16[128,1536]{1,0:T(8,128)(2,1)S(1)}, u32[]{:S(2)}, u32[]{:S(2)}) collective-permute-start(bf16[128,1536]{1,0:T(8,128)(2,1)} %collective-permute-done.50.refs_6_.refs_5_), channel_id=1, source_target_pairs={{0,4},{4,8},{8,12},{12,14},{14,10},{10,6},{6,2},{2,0},{1,5},{5,9},... | collective-permute-start | bytes 1179656 | tf_op jit(solution)/shard_map/ppermute | solution.py:297
  403.0 64.6 %collective-permute-start.53 = (bf16[128,1536]{1,0:T(8,128)(2,1)}, bf16[128,1536]{1,0:T(8,128)(2,1)S(1)}, u32[]{:S(2)}, u32[]{:S(2)}) collective-permute-start(bf16[128,1536]{1,0:T(8,128)(2,1)} %collective-permute-done.42.refs_9_.refs_8_), channel_id=1, source_target_pairs={{0,4},{4,8},{8,12},{12,14},{14,10},{10,6},{6,2},{2,0},{1,5},{5,9},... | collective-permute-start | bytes 1179656 | tf_op jit(solution)/shard_map/ppermute | solution.py:297
  404.6 63.1 %collective-permute-start.52 = (bf16[128,1536]{1,0:T(8,128)(2,1)}, bf16[128,1536]{1,0:T(8,128)(2,1)S(1)}, u32[]{:S(2)}, u32[]{:S(2)}) collective-permute-start(bf16[128,1536]{1,0:T(8,128)(2,1)} %collective-permute-done.49.refs_3_.refs_2_), channel_id=1, source_target_pairs={{4,0},{8,4},{12,8},{14,12},{10,14},{6,10},{2,6},{0,2},{5,1},{9,5},... | collective-permute-start | bytes 1179656 | tf_op jit(solution)/shard_map/ppermute | solution.py:301
  435.9 36.5 %collective-permute-start.46 = (bf16[512,1280]{1,0:T(8,128)(2,1)S(1)}, bf16[512,1280]{1,0:T(8,128)(2,1)S(1)}, u32[]{:S(2)}, u32[]{:S(2)}) collective-permute-start(bf16[512,1280]{1,0:T(8,128)(2,1)S(1)} %get-tuple-element.36), channel_id=1, source_target_pairs={{0,1},{1,0},{2,3},{3,2},{4,5},{5,4},{6,7},{7,6},{8,9},{9,8},{10,11... | collective-permute-start | bytes 3932168 | tf_op jit(solution)/shard_map/ppermute | solution.py:318
  472.6 48.1 %collective-permute-start.47 = (bf16[512,1280]{1,0:T(8,128)(2,1)S(1)}, bf16[512,1280]{1,0:T(8,128)(2,1)S(1)}, u32[]{:S(2)}, u32[]{:S(2)}) collective-permute-start(bf16[512,1280]{1,0:T(8,128)(2,1)S(1)} %add_convert_fusion.1), channel_id=1, source_target_pairs={{0,16},{16,0},{1,17},{17,1},{2,18},{18,2},{3,19},{19,3},{4,20},{20... | collective-permute-start | bytes 3932168 | tf_op jit(solution)/shard_map/ppermute | solution.py:318
  478.4 42.3 %collective-permute-start.56 = (bf16[512,768]{1,0:T(8,128)(2,1)S(1)}, bf16[512,768]{1,0:T(8,128)(2,1)S(1)}, u32[]{:S(2)}, u32[]{:S(2)}) collective-permute-start(bf16[512,768]{1,0:T(8,128)(2,1)S(1)} %add_convert_fusion.2), channel_id=1, source_target_pairs={{0,16},{16,0},{1,17},{17,1},{2,18},{18,2},{3,19},{19,3},{4,20},{20... | collective-permute-start | bytes 2359304 | tf_op jit(solution)/shard_map/ppermute | solution.py:318
  (75 other events, 1068.4 us)
where the time goes:
time: 528 us; the launch traced here: 524 us
  waiting for transfers between devices  307 us (58%)
  Pallas kernels  127 us (24%)
  starting transfers between devices  54.6 us (10%)
  local copies, waits for them, and re-layouts  28.9 us (5%)
    ppermute x15, waiting for transfers between devices, swap(): return lax.ppermute(array, axis, [(0, 1), (1, 0)])  129 us
    ppermute x21, waiting for transfers between devices, __init__(): down = lax.ppermute(down, 'fs', behind)  110 us
    ppermute x21, waiting for transfers between devices, __init__(): up = lax.ppermute(up, 'fs', ahead)  68.5 us
    pallas_call x3, Pallas kernels, hidden_rows(): pl.pallas_call(body, out_shape=jax.ShapeDtypeStruct((2 * part_rows, colum...  42.7 us
    pallas_call x6, Pallas kernels, project_back(): pl.pallas_call(body, out_shape=(part, part), grid=(2 * tiles,), in_specs=...  33 us
    pallas_call x4, Pallas kernels, project_rows(): pl.pallas_call(body, out_shape=jax.ShapeDtypeStruct((count * part_rows, c...  31.2 us
    ppermute x21, starting transfers between devices, __init__(): up = lax.ppermute(up, 'fs', ahead)  31.2 us
    unnamed x100, local copies, waits for them, and re-layouts  24.1 us
  transfers between devices with their start and end apart: 57, of which 23 were waited for; matrix products, arithmetic and copies ran while one was open for 2% of the time, Pallas kernels for 23%

commit v1 on v0

--- a/solution.py
+++ b/solution.py
@@ -415,7 +415,8 @@
     )(swapped, log_gamma, query_key, query_key, value_gate, value_gate, cosine, sine, gain.reshape(1, -1))
 
 
-VMEM_LIMIT = 26 * 2**20
+VMEM_LIMIT = 16 * 2**20
+HIDDEN_VMEM_LIMIT = 28 * 2**20
 
 
 def stacked(refs):
@@ -564,7 +565,7 @@
             + [strip_at(TAPS), strip_at(1)],
             out_specs=strip_at(2 * part_rows, 0),
         ),
-        compiler_params=pltpu.CompilerParams(vmem_limit_bytes=VMEM_LIMIT),
+        compiler_params=pltpu.CompilerParams(vmem_limit_bytes=HIDDEN_VMEM_LIMIT),
         cost_estimate=pl.CostEstimate(
             flops=8 * part_rows * depth * columns,
             bytes_accessed=4 * (part_rows * (depth + columns) + depth * columns),
@@ -734,6 +735,11 @@
     head_ids = (first_head + jnp.arange(heads, dtype=jnp.int32)).astype(jnp.float32)
     log_gamma = jnp.log(1.0 - 2.0 ** (-5.0 - head_ids))
     gain_dev = lax.dynamic_slice_in_dim(head_gain, first_head * HEAD_DIM, cols, 0)
+    first_hidden = (tp_index * 2 + rep_index) * hidden_cols
+
+    taps = lax.dynamic_slice_in_dim(filter_taps, first_hidden, hidden_cols, 1)
+    bias = lax.dynamic_slice_in_dim(filter_bias, first_hidden, hidden_cols, 0)[None, :]
+    gain_dev, taps, bias = lax.optimization_barrier((gain_dev, taps, bias))
     tables = (jnp.cos(angles), jnp.sin(angles), gain_dev, log_gamma, swapped)
     early_blocks, late_blocks = ring_a.parts(every), ring_b.parts(every)
 
@@ -754,10 +760,6 @@
     own_mid = [normed_mid, swap(normed_mid, "tp")]
     other_mid = [far, swap(far, "tp")]
 
-    first_hidden = (tp_index * 2 + rep_index) * hidden_cols
-
-    taps = lax.dynamic_slice_in_dim(filter_taps, first_hidden, hidden_cols, 1)
-    bias = lax.dynamic_slice_in_dim(filter_bias, first_hidden, hidden_cols, 0)[None, :]
     hidden_blocks = ring_g.parts(every), ring_l.parts(every)
 
     def hidden_strips(rows_in, shares):
@@ -766,7 +768,7 @@
             for share in range(shares)
         ]
 
-    own_hidden = hidden_strips(own_mid, 2)
+    own_hidden = hidden_strips(own_mid, 1)
     other_hidden = hidden_strips(other_mid, 1)
     near = count // 2 - 2
     groups = [

time: 528 us -> 514 us (0.973)
  Pallas kernels: 127 us -> 115 us
  waiting for transfers between devices: 307 us -> 316 us
  local copies, waits for them, and re-layouts: 28.9 us -> 23.2 us
    pallas_call x3 -> x2, Pallas kernels: 42.7 us -> 35.7 us  [hidden_rows(): pl.pallas_call(body, out_shape=jax.ShapeDtypeStruct((2 * part_rows, colum...]
    unnamed x100 -> x68, local copies, waits for them, and re-layouts: 24.1 us -> 18.4 us
  transfers between devices with their start and end apart: 57 -> 57, of which waited for: 23 -> 23; matrix products, arithmetic and copies ran while one was open for 2% -> 2% of each run, Pallas kernels for 23% -> 21%
where the time goes in v1:
time: 514 us
  waiting for transfers between devices  316 us (61%)
  Pallas kernels  115 us (22%)
  starting transfers between devices  54.4 us (11%)
  local copies, waits for them, and re-layouts  23.2 us (5%)
    ppermute x15, waiting for transfers between devices, swap(): return lax.ppermute(array, axis, [(0, 1), (1, 0)])  131 us
    ppermute x21, waiting for transfers between devices, __init__(): down = lax.ppermute(down, 'fs', behind)  113 us
    ppermute x21, waiting for transfers between devices, __init__(): up = lax.ppermute(up, 'fs', ahead)  72.2 us
    pallas_call x2, Pallas kernels, hidden_rows(): pl.pallas_call(body, out_shape=jax.ShapeDtypeStruct((2 * part_rows, colum...  35.7 us
    ppermute x21, starting transfers between devices, __init__(): up = lax.ppermute(up, 'fs', ahead)  31.1 us
    pallas_call x4, Pallas kernels, project_rows(): pl.pallas_call(body, out_shape=jax.ShapeDtypeStruct((count * part_rows, c...  31 us
    pallas_call x6, Pallas kernels, project_back(): pl.pallas_call(body, out_shape=(part, part), grid=(2 * tiles,), in_specs=...  28.2 us
    unnamed x68, local copies, waits for them, and re-layouts  18.4 us
  transfers between devices with their start and end apart: 57, of which 23 were waited for; matrix products, arithmetic and copies ran while one was open for 2% of the time, Pallas kernels for 21%

profile of v1, /device:TPU:0, one launch (start us, length us, event | category | flops | bytes accessed | tf_op | source)
XLA Modules:
  0.0 513.7 jit_solution(3015985373206063597)
XLA Ops:
  11.3 43.0 %collective-permute-done.16.refs_0_ = bf16[512,2048]{1,0:T(8,128)(2,1)} collective-permute-done((bf16[512,2048]{1,0:T(8,128)(2,1)}, bf16[512,2048]{1,0:T(8,128)(2,1)}, u32[]{:S(2)}, u32[]{:S(2)}) %collective-permute-start.16) | collective-permute-done | bytes 2097184 | tf_op jit(solution)/shard_map/ppermute | solution.py:318
  59.2 15.6 %collective-permute-done.12.refs_9_.refs_8_ = bf16[256,1536]{1,0:T(8,128)(2,1)} collective-permute-done((bf16[256,1536]{1,0:T(8,128)(2,1)S(1)}, bf16[256,1536]{1,0:T(8,128)(2,1)}, u32[]{:S(2)}, u32[]{:S(2)}) %collective-permute-start.12) | collective-permute-done | bytes 786464 | tf_op jit(solution)/shard_map/ppermute | solution.py:297
  76.8 11.0 %collective-permute-done.1.refs_3_ = bf16[256,1024]{1,0:T(8,128)(2,1)} collective-permute-done((bf16[256,1024]{1,0:T(8,128)(2,1)S(1)}, bf16[256,1024]{1,0:T(8,128)(2,1)}, u32[]{:S(2)}, u32[]{:S(2)}) %collective-permute-start.1) | collective-permute-done | bytes 524320 | tf_op jit(solution)/shard_map/ppermute | solution.py:301
  89.9 25.3 %collective-permute-done.2.refs_4_ = bf16[256,1024]{1,0:T(8,128)(2,1)} collective-permute-done((bf16[256,1024]{1,0:T(8,128)(2,1)}, bf16[256,1024]{1,0:T(8,128)(2,1)}, u32[]{:S(2)}, u32[]{:S(2)}) %collective-permute-start.2) | collective-permute-done | bytes 524320 | tf_op jit(solution)/shard_map/ppermute | solution.py:301
  123.5 6.8 %collective-permute-done.3.refs_5_ = bf16[256,1024]{1,0:T(8,128)(2,1)} collective-permute-done((bf16[256,1024]{1,0:T(8,128)(2,1)}, bf16[256,1024]{1,0:T(8,128)(2,1)}, u32[]{:S(2)}, u32[]{:S(2)}) %collective-permute-start.3) | collective-permute-done | bytes 524320 | tf_op jit(solution)/shard_map/ppermute | solution.py:301
  130.6 8.2 %shard_map.141.query_ref.key_ref = bf16[1024,1024]{1,0:T(8,128)(2,1)S(1)} custom-call(bf16[512,2048]{1,0:T(8,128)(2,1)} %collective-permute-done.16.refs_0_, bf16[512,2048]{1,0:T(8,128)(2,1)} %collective-permute-done.17.refs_1_, bf16[256,1024]{1,0:T(8,128)(2,1)S(1)} %pad_maximum_fusion.1.refs_2_, bf16[256,1024]{1,0:T(8,128)(2,1)} %collective-permute-done.1.refs_3_, ...), custom_call_target="tpu_custom_call" | custom-call | flops 4294967296 | bytes 10485760 | tf_op jit(solution)/shard_map/pallas_call | solution.py:448
  138.8 6.8 %collective-permute-done.14.refs_7_.refs_6_ = bf16[256,1536]{1,0:T(8,128)(2,1)} collective-permute-done((bf16[256,1536]{1,0:T(8,128)(2,1)}, bf16[256,1536]{1,0:T(8,128)(2,1)}, u32[]{:S(2)}, u32[]{:S(2)}) %collective-permute-start.14) | collective-permute-done | bytes 786464 | tf_op jit(solution)/shard_map/ppermute | solution.py:297
  145.7 8.0 %shard_map.142.value_ref.gate_ref = bf16[1024,1024]{1,0:T(8,128)(2,1)S(1)} custom-call(bf16[512,2048]{1,0:T(8,128)(2,1)} %collective-permute-done.16.refs_0_, bf16[512,2048]{1,0:T(8,128)(2,1)} %collective-permute-done.17.refs_1_, bf16[256,1536]{1,0:T(8,128)(2,1)S(1)} %pad_maximum_fusion.refs_2_.refs_1_, bf16[256,1536]{1,0:T(8,128)(2,1)S(1)} %copy-done.28, ...), custom_call_target="tpu_custom_call" | custom-call | flops 4294967296 | bytes 10485760 | tf_op jit(solution)/shard_map/pallas_call | solution.py:448
  153.7 5.1 shard_map.143.refs_0_
  158.8 4.9 shard_map.144
  163.8 7.4 %shard_map.137.query_ref.key_ref = bf16[1024,1024]{1,0:T(8,128)(2,1)S(1)} custom-call(bf16[512,2048]{1,0:T(8,128)(2,1)} %shard_map.136.refs_0_, bf16[512,2048]{1,0:T(8,128)(2,1)S(1)} %collective-permute-done.refs_1_, bf16[256,1024]{1,0:T(8,128)(2,1)S(1)} %pad_maximum_fusion.1.refs_2_, bf16[256,1024]{1,0:T(8,128)(2,1)} %collective-permute-done.1.refs_3_, ...), custom_call_target="tpu_custom_call" | custom-call | flops 4294967296 | bytes 10485760 | tf_op jit(solution)/shard_map/pallas_call | solution.py:448
  171.2 7.4 %shard_map.138.value_ref.gate_ref = bf16[1024,1024]{1,0:T(8,128)(2,1)S(1)} custom-call(bf16[512,2048]{1,0:T(8,128)(2,1)} %shard_map.136.refs_0_, bf16[512,2048]{1,0:T(8,128)(2,1)S(1)} %collective-permute-done.refs_1_, bf16[256,1536]{1,0:T(8,128)(2,1)S(1)} %pad_maximum_fusion.refs_2_.refs_1_, bf16[256,1536]{1,0:T(8,128)(2,1)S(1)} %copy-done.28, ...), custom_call_target="tpu_custom_call" | custom-call | flops 4294967296 | bytes 10485760 | tf_op jit(solution)/shard_map/pallas_call | solution.py:448
  178.6 5.1 shard_map.139.refs_0_
  183.7 5.9 %shard_map.140 = (bf16[512,2048]{1,0:T(8,128)(2,1)S(1)}, bf16[512,2048]{1,0:T(8,128)(2,1)}) custom-call(bf16[1024,512]{1,0:T(8,128)(2,1)S(1)} %shard_map.139.refs_0_, bf16[256,1536]{1,0:T(8,128)(2,1)S(1)} %pad_maximum_fusion.refs_2_.refs_1_, bf16[256,1536]{1,0:T(8,128)(2,1)S(1)} %copy-done.28, bf16[256,1536]{1,0:T(8,128)(2,1)} %collective-permute-done.9.refs_4_.refs_3_, ...), custom_call_target="tpu_custom_call" | custom-call | flops 2147483648 | bytes 7340032 | tf_op jit(solution)/shard_map/pallas_call | solution.py:485
  198.6 42.9 %collective-permute-done.19.far_ref = bf16[512,2048]{1,0:T(8,128)(2,1)} collective-permute-done((bf16[512,2048]{1,0:T(8,128)(2,1)}, bf16[512,2048]{1,0:T(8,128)(2,1)}, u32[]{:S(2)}, u32[]{:S(2)}) %collective-permute-start.19) | collective-permute-done | bytes 2097184 | tf_op jit(solution)/shard_map/ppermute | solution.py:318
  243.1 4.5 shard_map.145
  256.1 15.5 %collective-permute-done.25.refs_6_ = bf16[256,1536]{1,0:T(8,128)(2,1)S(1)} collective-permute-done((bf16[256,1536]{1,0:T(8,128)(2,1)S(1)}, bf16[256,1536]{1,0:T(8,128)(2,1)S(1)}, u32[]{:S(2)}, u32[]{:S(2)}) %collective-permute-start.25) | collective-permute-done | bytes 786464 | tf_op jit(solution)/shard_map/ppermute | solution.py:297
  275.4 14.6 %collective-permute-done.21.refs_1_ = bf16[256,1536]{1,0:T(8,128)(2,1)S(1)} collective-permute-done((bf16[256,1536]{1,0:T(8,128)(2,1)S(1)}, bf16[256,1536]{1,0:T(8,128)(2,1)S(1)}, u32[]{:S(2)}, u32[]{:S(2)}) %collective-permute-start.21) | collective-permute-done | bytes 786464 | tf_op jit(solution)/shard_map/ppermute | solution.py:301
  296.4 9.0 %collective-permute-done.26.refs_5_ = bf16[256,1536]{1,0:T(8,128)(2,1)} collective-permute-done((bf16[256,1536]{1,0:T(8,128)(2,1)S(1)}, bf16[256,1536]{1,0:T(8,128)(2,1)}, u32[]{:S(2)}, u32[]{:S(2)}) %collective-permute-start.26) | collective-permute-done | bytes 786464 | tf_op jit(solution)/shard_map/ppermute | solution.py:297
  307.4 16.4 %collective-permute-done.22.refs_2_ = bf16[256,1536]{1,0:T(8,128)(2,1)} collective-permute-done((bf16[256,1536]{1,0:T(8,128)(2,1)S(1)}, bf16[256,1536]{1,0:T(8,128)(2,1)}, u32[]{:S(2)}, u32[]{:S(2)}) %collective-permute-start.22) | collective-permute-done | bytes 786464 | tf_op jit(solution)/shard_map/ppermute | solution.py:301
  327.0 12.1 %collective-permute-done.27.refs_4_ = bf16[256,1536]{1,0:T(8,128)(2,1)} collective-permute-done((bf16[256,1536]{1,0:T(8,128)(2,1)}, bf16[256,1536]{1,0:T(8,128)(2,1)}, u32[]{:S(2)}, u32[]{:S(2)}) %collective-permute-start.27) | collective-permute-done | bytes 786464 | tf_op jit(solution)/shard_map/ppermute | solution.py:297
  342.2 15.3 %collective-permute-done.23.refs_3_ = bf16[256,1536]{1,0:T(8,128)(2,1)} collective-permute-done((bf16[256,1536]{1,0:T(8,128)(2,1)}, bf16[256,1536]{1,0:T(8,128)(2,1)}, u32[]{:S(2)}, u32[]{:S(2)}) %collective-permute-start.23) | collective-permute-done | bytes 786464 | tf_op jit(solution)/shard_map/ppermute | solution.py:301
  357.9 7.8 %collective-permute-done.35.refs_3_ = bf16[128,1536]{1,0:T(8,128)(2,1)S(1)} collective-permute-done((bf16[128,1536]{1,0:T(8,128)(2,1)S(1)}, bf16[128,1536]{1,0:T(8,128)(2,1)S(1)}, u32[]{:S(2)}, u32[]{:S(2)}) %collective-permute-start.35) | collective-permute-done | bytes 393248 | tf_op jit(solution)/shard_map/ppermute | solution.py:301
  369.4 4.8 collective-permute-done.36.refs_4_
  374.7 8.0 %collective-permute-done.37.refs_5_ = bf16[128,1536]{1,0:T(8,128)(2,1)S(1)} collective-permute-done((bf16[128,1536]{1,0:T(8,128)(2,1)S(1)}, bf16[128,1536]{1,0:T(8,128)(2,1)S(1)}, u32[]{:S(2)}, u32[]{:S(2)}) %collective-permute-start.37) | collective-permute-done | bytes 393248 | tf_op jit(solution)/shard_map/ppermute | solution.py:301
  389.2 5.4 %collective-permute-done.50.refs_5_ = bf16[128,1536]{1,0:T(8,128)(2,1)S(1)} collective-permute-done((bf16[128,1536]{1,0:T(8,128)(2,1)S(1)}, bf16[128,1536]{1,0:T(8,128)(2,1)S(1)}, u32[]{:S(2)}, u32[]{:S(2)}) %collective-permute-start.50) | collective-permute-done | bytes 393248 | tf_op jit(solution)/shard_map/ppermute | solution.py:297
  395.1 7.5 %collective-permute-done.42.refs_8_ = bf16[128,1536]{1,0:T(8,128)(2,1)S(1)} collective-permute-done((bf16[128,1536]{1,0:T(8,128)(2,1)S(1)}, bf16[128,1536]{1,0:T(8,128)(2,1)S(1)}, u32[]{:S(2)}, u32[]{:S(2)}) %collective-permute-start.42) | collective-permute-done | bytes 393248 | tf_op jit(solution)/shard_map/ppermute | solution.py:297
  411.9 18.1 %shard_map.148.refs_0_ = bf16[1024,1536]{1,0:T(8,128)(2,1)S(1)} custom-call(s32[1]{0:T(128)} %bitcast.swapped_ref, bf16[512,2048]{1,0:T(8,128)(2,1)} %collective-permute-done.44.mine_ref, bf16[512,2048]{1,0:T(8,128)(2,1)} %collective-permute-done.45.theirs_ref, bf16[256,1536]{1,0:T(8,128)(2,1)S(1)} %constant_dynamic-slice_fusion.2.refs_0_, ...), custom_call_target="tpu_custom_call" | custom-call | flops 12884901888 | bytes 19922944 | tf_op jit(solution)/shard_map/pallas_call | solution.py:557
  430.1 5.1 %shard_map.149 = (bf16[512,1280]{1,0:T(8,128)(2,1)S(1)}, bf16[512,1280]{1,0:T(8,128)(2,1)S(1)}) custom-call(bf16[1024,1536]{1,0:T(8,128)(2,1)S(1)} %shard_map.148.refs_0_, bf16[128,1536]{1,0:T(8,128)(2,1)S(1)} %get-tuple-element.37.refs_1_, bf16[128,1536]{1,0:T(8,128)(2,1)S(1)} %get-tuple-element.38.refs_2_, ...), custom_call_target="tpu_custom_call" | custom-call | flops 4026531840 | bytes 9699328 | tf_op jit(solution)/shard_map/pallas_call | solution.py:485
  435.4 17.5 %shard_map.146.refs_0_ = bf16[1024,1536]{1,0:T(8,128)(2,1)S(1)} custom-call(s32[1]{0:T(128)} %bitcast.swapped_ref, bf16[512,2048]{1,0:T(8,128)(2,1)S(1)} %copy-done.11, bf16[512,2048]{1,0:T(8,128)(2,1)S(1)} %collective-permute-done.20.theirs_ref, bf16[256,1536]{1,0:T(8,128)(2,1)S(1)} %constant_dynamic-slice_fusion.2.refs_0_, ...), custom_call_target="tpu_custom_call" | custom-call | flops 12884901888 | bytes 19922944 | tf_op jit(solution)/shard_map/pallas_call | solution.py:557
  452.9 5.4 %shard_map.147 = (bf16[512,1280]{1,0:T(8,128)(2,1)S(1)}, bf16[512,1280]{1,0:T(8,128)(2,1)S(1)}) custom-call(bf16[1024,1536]{1,0:T(8,128)(2,1)S(1)} %shard_map.146.refs_0_, bf16[128,1536]{1,0:T(8,128)(2,1)S(1)} %get-tuple-element.37.refs_1_, bf16[128,1536]{1,0:T(8,128)(2,1)S(1)} %get-tuple-element.38.refs_2_, ...), custom_call_target="tpu_custom_call" | custom-call | flops 4026531840 | bytes 9699328 | tf_op jit(solution)/shard_map/pallas_call | solution.py:485
  469.1 41.7 %collective-permute-done.56.refs_5_ = bf16[512,768]{1,0:T(8,128)(2,1)S(1)} collective-permute-done((bf16[512,768]{1,0:T(8,128)(2,1)S(1)}, bf16[512,768]{1,0:T(8,128)(2,1)S(1)}, u32[]{:S(2)}, u32[]{:S(2)}) %collective-permute-start.56) | collective-permute-done | bytes 786464 | tf_op jit(solution)/shard_map/ppermute | solution.py:318
  (186 shorter events, 101.2 us)
Async XLA Ops:
  5.4 48.9 %collective-permute-start.16 = (bf16[512,2048]{1,0:T(8,128)(2,1)}, bf16[512,2048]{1,0:T(8,128)(2,1)}, u32[]{:S(2)}, u32[]{:S(2)}) collective-permute-start(bf16[512,2048]{1,0:T(8,128)(2,1)} %shard_map.136.refs_0_), channel_id=1, source_target_pairs={{0,16},{16,0},{1,17},{17,1},{2,18},{18,2},{3,19},{19,3},{4,20},{20... | collective-permute-start | bytes 6291464 | tf_op jit(solution)/shard_map/ppermute | solution.py:318
  8.5 47.6 %collective-permute-start.8 = (bf16[256,1536]{1,0:T(8,128)(2,1)S(1)}, bf16[256,1536]{1,0:T(8,128)(2,1)S(1)}, u32[]{:S(2)}, u32[]{:S(2)}) collective-permute-start(bf16[256,1536]{1,0:T(8,128)(2,1)S(1)} %pad_maximum_fusion.refs_2_.refs_1_), channel_id=1, source_target_pairs={{4,0},{8,4},{12,8},{14,12},{10,14},{6,10},{2,6},{0,2},{5,1},{9,5},... | collective-permute-start | bytes 2359304 | tf_op jit(solution)/shard_map/ppermute | solution.py:301
  10.2 48.8 %collective-permute-start.4 = (bf16[256,1024]{1,0:T(8,128)(2,1)S(1)}, bf16[256,1024]{1,0:T(8,128)(2,1)S(1)}, u32[]{:S(2)}, u32[]{:S(2)}) collective-permute-start(bf16[256,1024]{1,0:T(8,128)(2,1)S(1)} %pad_maximum_fusion.1.refs_2_), channel_id=1, source_target_pairs={{0,4},{4,8},{8,12},{12,14},{14,10},{10,6},{6,2},{2,0},{1,5},{5,9},... | collective-permute-start | bytes 1572872 | tf_op jit(solution)/shard_map/ppermute | solution.py:297
  54.3 76.3 %collective-permute-start.17 = (bf16[512,2048]{1,0:T(8,128)(2,1)}, bf16[512,2048]{1,0:T(8,128)(2,1)}, u32[]{:S(2)}, u32[]{:S(2)}) collective-permute-start(bf16[512,2048]{1,0:T(8,128)(2,1)} %collective-permute-done.16.refs_0_), channel_id=1, source_target_pairs={{0,1},{1,0},{2,3},{3,2},{4,5},{5,4},{6,7},{7,6},{8,9},{9,8},{10,11... | collective-permute-start | bytes 6291464 | tf_op jit(solution)/shard_map/ppermute | solution.py:318
  57.2 30.7 %collective-permute-start.1 = (bf16[256,1024]{1,0:T(8,128)(2,1)S(1)}, bf16[256,1024]{1,0:T(8,128)(2,1)}, u32[]{:S(2)}, u32[]{:S(2)}) collective-permute-start(bf16[256,1024]{1,0:T(8,128)(2,1)S(1)} %pad_maximum_fusion.1.refs_2_), channel_id=1, source_target_pairs={{4,0},{8,4},{12,8},{14,12},{10,14},{6,10},{2,6},{0,2},{5,1},{9,5},... | collective-permute-start | bytes 1572872 | tf_op jit(solution)/shard_map/ppermute | solution.py:301
  59.0 29.1 %collective-permute-start.5 = (bf16[256,1024]{1,0:T(8,128)(2,1)S(1)}, bf16[256,1024]{1,0:T(8,128)(2,1)}, u32[]{:S(2)}, u32[]{:S(2)}) collective-permute-start(bf16[256,1024]{1,0:T(8,128)(2,1)S(1)} %collective-permute-done.4.refs_9_), channel_id=1, source_target_pairs={{0,4},{4,8},{8,12},{12,14},{14,10},{10,6},{6,2},{2,0},{1,5},{5,9},... | collective-permute-start | bytes 1572872 | tf_op jit(solution)/shard_map/ppermute | solution.py:297
  74.8 43.2 %collective-permute-start.13 = (bf16[256,1536]{1,0:T(8,128)(2,1)}, bf16[256,1536]{1,0:T(8,128)(2,1)}, u32[]{:S(2)}, u32[]{:S(2)}) collective-permute-start(bf16[256,1536]{1,0:T(8,128)(2,1)} %collective-permute-done.12.refs_9_.refs_8_), channel_id=1, source_target_pairs={{0,4},{4,8},{8,12},{12,14},{14,10},{10,6},{6,2},{2,0},{1,5},{5,9},... | collective-permute-start | bytes 2359304 | tf_op jit(solution)/shard_map/ppermute | solution.py:297
  76.6 42.9 %collective-permute-start.10 = (bf16[256,1536]{1,0:T(8,128)(2,1)}, bf16[256,1536]{1,0:T(8,128)(2,1)}, u32[]{:S(2)}, u32[]{:S(2)}) collective-permute-start(bf16[256,1536]{1,0:T(8,128)(2,1)} %collective-permute-done.9.refs_4_.refs_3_), channel_id=1, source_target_pairs={{4,0},{8,4},{12,8},{14,12},{10,14},{6,10},{2,6},{0,2},{5,1},{9,5},... | collective-permute-start | bytes 2359304 | tf_op jit(solution)/shard_map/ppermute | solution.py:301
  118.0 27.7 %collective-permute-start.14 = (bf16[256,1536]{1,0:T(8,128)(2,1)}, bf16[256,1536]{1,0:T(8,128)(2,1)}, u32[]{:S(2)}, u32[]{:S(2)}) collective-permute-start(bf16[256,1536]{1,0:T(8,128)(2,1)} %collective-permute-done.13.refs_8_.refs_7_), channel_id=1, source_target_pairs={{0,4},{4,8},{8,12},{12,14},{14,10},{10,6},{6,2},{2,0},{1,5},{5,9},... | collective-permute-start | bytes 2359304 | tf_op jit(solution)/shard_map/ppermute | solution.py:297
  130.3 33.5 %collective-permute-start = (bf16[512,2048]{1,0:T(8,128)(2,1)}, bf16[512,2048]{1,0:T(8,128)(2,1)S(1)}, u32[]{:S(2)}, u32[]{:S(2)}) collective-permute-start(bf16[512,2048]{1,0:T(8,128)(2,1)} %shard_map.136.refs_0_), channel_id=1, source_target_pairs={{0,1},{1,0},{2,3},{3,2},{4,5},{5,4},{6,7},{7,6},{8,9},{9,8},{10,11... | collective-permute-start | bytes 6291464 | tf_op jit(solution)/shard_map/ppermute | solution.py:318
  193.6 47.9 %collective-permute-start.19 = (bf16[512,2048]{1,0:T(8,128)(2,1)}, bf16[512,2048]{1,0:T(8,128)(2,1)}, u32[]{:S(2)}, u32[]{:S(2)}) collective-permute-start(bf16[512,2048]{1,0:T(8,128)(2,1)} %add_convert_fusion), channel_id=1, source_target_pairs={{0,16},{16,0},{1,17},{17,1},{2,18},{18,2},{3,19},{19,3},{4,20},{20... | collective-permute-start | bytes 6291464 | tf_op jit(solution)/shard_map/ppermute | solution.py:318
  195.2 55.9 %collective-permute-start.24 = (bf16[256,1536]{1,0:T(8,128)(2,1)S(1)}, bf16[256,1536]{1,0:T(8,128)(2,1)S(1)}, u32[]{:S(2)}, u32[]{:S(2)}) collective-permute-start(bf16[256,1536]{1,0:T(8,128)(2,1)S(1)} %constant_dynamic-slice_fusion.2.refs_0_), channel_id=1, source_target_pairs={{0,4},{4,8},{8,12},{12,14},{14,10},{10,6},{6,2},{2,0},{1,5},{5,9},... | collective-permute-start | bytes 2359304 | tf_op jit(solution)/shard_map/ppermute | solution.py:297
  198.0 54.7 %collective-permute-start.28 = (bf16[256,1536]{1,0:T(8,128)(2,1)S(1)}, bf16[256,1536]{1,0:T(8,128)(2,1)S(1)}, u32[]{:S(2)}, u32[]{:S(2)}) collective-permute-start(bf16[256,1536]{1,0:T(8,128)(2,1)S(1)} %constant_dynamic-slice_fusion.1.refs_8_), channel_id=1, source_target_pairs={{4,0},{8,4},{12,8},{14,12},{10,14},{6,10},{2,6},{0,2},{5,1},{9,5},... | collective-permute-start | bytes 2359304 | tf_op jit(solution)/shard_map/ppermute | solution.py:301
  249.5 46.8 %collective-permute-start.44 = (bf16[512,2048]{1,0:T(8,128)(2,1)S(1)}, bf16[512,2048]{1,0:T(8,128)(2,1)}, u32[]{:S(2)}, u32[]{:S(2)}) collective-permute-start(bf16[512,2048]{1,0:T(8,128)(2,1)S(1)} %get-tuple-element.32.mine_ref), channel_id=1, source_target_pairs={{0,16},{16,0},{1,17},{17,1},{2,18},{18,2},{3,19},{19,3},{4,20},{20... | collective-permute-start | bytes 6291464 | tf_op jit(solution)/shard_map/ppermute | solution.py:318
  254.0 35.9 %collective-permute-start.21 = (bf16[256,1536]{1,0:T(8,128)(2,1)S(1)}, bf16[256,1536]{1,0:T(8,128)(2,1)S(1)}, u32[]{:S(2)}, u32[]{:S(2)}) collective-permute-start(bf16[256,1536]{1,0:T(8,128)(2,1)S(1)} %constant_dynamic-slice_fusion.2.refs_0_), channel_id=1, source_target_pairs={{4,0},{8,4},{12,8},{14,12},{10,14},{6,10},{2,6},{0,2},{5,1},{9,5},... | collective-permute-start | bytes 2359304 | tf_op jit(solution)/shard_map/ppermute | solution.py:301
  255.6 35.8 %collective-permute-start.32 = (bf16[256,1536]{1,0:T(8,128)(2,1)S(1)}, bf16[256,1536]{1,0:T(8,128)(2,1)S(1)}, u32[]{:S(2)}, u32[]{:S(2)}) collective-permute-start(bf16[256,1536]{1,0:T(8,128)(2,1)S(1)} %constant_dynamic-slice_fusion.1.refs_8_), channel_id=1, source_target_pairs={{0,4},{4,8},{8,12},{12,14},{14,10},{10,6},{6,2},{2,0},{1,5},{5,9},... | collective-permute-start | bytes 2359304 | tf_op jit(solution)/shard_map/ppermute | solution.py:297
  271.5 33.8 %collective-permute-start.26 = (bf16[256,1536]{1,0:T(8,128)(2,1)S(1)}, bf16[256,1536]{1,0:T(8,128)(2,1)}, u32[]{:S(2)}, u32[]{:S(2)}) collective-permute-start(bf16[256,1536]{1,0:T(8,128)(2,1)S(1)} %collective-permute-done.25.refs_6_), channel_id=1, source_target_pairs={{0,4},{4,8},{8,12},{12,14},{14,10},{10,6},{6,2},{2,0},{1,5},{5,9},... | collective-permute-start | bytes 2359304 | tf_op jit(solution)/shard_map/ppermute | solution.py:297
  274.0 32.9 %collective-permute-start.30 = (bf16[256,1536]{1,0:T(8,128)(2,1)S(1)}, bf16[256,1536]{1,0:T(8,128)(2,1)}, u32[]{:S(2)}, u32[]{:S(2)}) collective-permute-start(bf16[256,1536]{1,0:T(8,128)(2,1)S(1)} %collective-permute-done.29.refs_10_), channel_id=1, source_target_pairs={{4,0},{8,4},{12,8},{14,12},{10,14},{6,10},{2,6},{0,2},{5,1},{9,5},... | collective-permute-start | bytes 2359304 | tf_op jit(solution)/shard_map/ppermute | solution.py:301
  290.0 33.8 %collective-permute-start.22 = (bf16[256,1536]{1,0:T(8,128)(2,1)S(1)}, bf16[256,1536]{1,0:T(8,128)(2,1)}, u32[]{:S(2)}, u32[]{:S(2)}) collective-permute-start(bf16[256,1536]{1,0:T(8,128)(2,1)S(1)} %collective-permute-done.21.refs_1_), channel_id=1, source_target_pairs={{4,0},{8,4},{12,8},{14,12},{10,14},{6,10},{2,6},{0,2},{5,1},{9,5},... | collective-permute-start | bytes 2359304 | tf_op jit(solution)/shard_map/ppermute | solution.py:301
  291.3 32.9 %collective-permute-start.33 = (bf16[256,1536]{1,0:T(8,128)(2,1)S(1)}, bf16[256,1536]{1,0:T(8,128)(2,1)}, u32[]{:S(2)}, u32[]{:S(2)}) collective-permute-start(bf16[256,1536]{1,0:T(8,128)(2,1)S(1)} %collective-permute-done.32.refs_15_), channel_id=1, source_target_pairs={{0,4},{4,8},{8,12},{12,14},{14,10},{10,6},{6,2},{2,0},{1,5},{5,9},... | collective-permute-start | bytes 2359304 | tf_op jit(solution)/shard_map/ppermute | solution.py:297
  296.4 109.4 %collective-permute-start.45 = (bf16[512,2048]{1,0:T(8,128)(2,1)}, bf16[512,2048]{1,0:T(8,128)(2,1)}, u32[]{:S(2)}, u32[]{:S(2)}) collective-permute-start(bf16[512,2048]{1,0:T(8,128)(2,1)} %collective-permute-done.44.mine_ref), channel_id=1, source_target_pairs={{0,1},{1,0},{2,3},{3,2},{4,5},{5,4},{6,7},{7,6},{8,9},{9,8},{10,11... | collective-permute-start | bytes 6291464 | tf_op jit(solution)/shard_map/ppermute | solution.py:318
  305.4 33.7 %collective-permute-start.27 = (bf16[256,1536]{1,0:T(8,128)(2,1)}, bf16[256,1536]{1,0:T(8,128)(2,1)}, u32[]{:S(2)}, u32[]{:S(2)}) collective-permute-start(bf16[256,1536]{1,0:T(8,128)(2,1)} %collective-permute-done.26.refs_5_), channel_id=1, source_target_pairs={{0,4},{4,8},{8,12},{12,14},{14,10},{10,6},{6,2},{2,0},{1,5},{5,9},... | collective-permute-start | bytes 2359304 | tf_op jit(solution)/shard_map/ppermute | solution.py:297
  306.9 33.7 %collective-permute-start.31 = (bf16[256,1536]{1,0:T(8,128)(2,1)}, bf16[256,1536]{1,0:T(8,128)(2,1)}, u32[]{:S(2)}, u32[]{:S(2)}) collective-permute-start(bf16[256,1536]{1,0:T(8,128)(2,1)} %collective-permute-done.30.refs_11_), channel_id=1, source_target_pairs={{4,0},{8,4},{12,8},{14,12},{10,14},{6,10},{2,6},{0,2},{5,1},{9,5},... | collective-permute-start | bytes 2359304 | tf_op jit(solution)/shard_map/ppermute | solution.py:301
  323.8 33.7 %collective-permute-start.23 = (bf16[256,1536]{1,0:T(8,128)(2,1)}, bf16[256,1536]{1,0:T(8,128)(2,1)}, u32[]{:S(2)}, u32[]{:S(2)}) collective-permute-start(bf16[256,1536]{1,0:T(8,128)(2,1)} %collective-permute-done.22.refs_2_), channel_id=1, source_target_pairs={{4,0},{8,4},{12,8},{14,12},{10,14},{6,10},{2,6},{0,2},{5,1},{9,5},... | collective-permute-start | bytes 2359304 | tf_op jit(solution)/shard_map/ppermute | solution.py:301
  324.2 43.6 %collective-permute-start.34 = (bf16[256,1536]{1,0:T(8,128)(2,1)}, bf16[256,1536]{1,0:T(8,128)(2,1)}, u32[]{:S(2)}, u32[]{:S(2)}) collective-permute-start(bf16[256,1536]{1,0:T(8,128)(2,1)} %collective-permute-done.33.refs_14_), channel_id=1, source_target_pairs={{0,4},{4,8},{8,12},{12,14},{14,10},{10,6},{6,2},{2,0},{1,5},{5,9},... | collective-permute-start | bytes 2359304 | tf_op jit(solution)/shard_map/ppermute | solution.py:297
  382.6 52.6 %collective-permute-start.20 = (bf16[512,2048]{1,0:T(8,128)(2,1)}, bf16[512,2048]{1,0:T(8,128)(2,1)S(1)}, u32[]{:S(2)}, u32[]{:S(2)}) collective-permute-start(bf16[512,2048]{1,0:T(8,128)(2,1)} %copy-done.10), channel_id=1, source_target_pairs={{0,1},{1,0},{2,3},{3,2},{4,5},{5,4},{6,7},{7,6},{8,9},{9,8},{10,11... | collective-permute-start | bytes 6291464 | tf_op jit(solution)/shard_map/ppermute | solution.py:318
  394.6 63.7 %collective-permute-start.48 = (bf16[128,1536]{1,0:T(8,128)(2,1)S(1)}, bf16[128,1536]{1,0:T(8,128)(2,1)S(1)}, u32[]{:S(2)}, u32[]{:S(2)}) collective-permute-start(bf16[128,1536]{1,0:T(8,128)(2,1)S(1)} %collective-permute-done.37.refs_5_), channel_id=1, source_target_pairs={{4,0},{8,4},{12,8},{14,12},{10,14},{6,10},{2,6},{0,2},{5,1},{9,5},... | collective-permute-start | bytes 1179656 | tf_op jit(solution)/shard_map/ppermute | solution.py:301
  402.6 56.3 %collective-permute-start.51 = (bf16[128,1536]{1,0:T(8,128)(2,1)S(1)}, bf16[128,1536]{1,0:T(8,128)(2,1)S(1)}, u32[]{:S(2)}, u32[]{:S(2)}) collective-permute-start(bf16[128,1536]{1,0:T(8,128)(2,1)S(1)} %collective-permute-done.50.refs_5_), channel_id=1, source_target_pairs={{0,4},{4,8},{8,12},{12,14},{14,10},{10,6},{6,2},{2,0},{1,5},{5,9},... | collective-permute-start | bytes 1179656 | tf_op jit(solution)/shard_map/ppermute | solution.py:297
  404.2 54.7 %collective-permute-start.53 = (bf16[128,1536]{1,0:T(8,128)(2,1)S(1)}, bf16[128,1536]{1,0:T(8,128)(2,1)S(1)}, u32[]{:S(2)}, u32[]{:S(2)}) collective-permute-start(bf16[128,1536]{1,0:T(8,128)(2,1)S(1)} %collective-permute-done.42.refs_8_), channel_id=1, source_target_pairs={{0,4},{4,8},{8,12},{12,14},{14,10},{10,6},{6,2},{2,0},{1,5},{5,9},... | collective-permute-start | bytes 1179656 | tf_op jit(solution)/shard_map/ppermute | solution.py:297
  405.8 53.1 %collective-permute-start.52 = (bf16[128,1536]{1,0:T(8,128)(2,1)S(1)}, bf16[128,1536]{1,0:T(8,128)(2,1)S(1)}, u32[]{:S(2)}, u32[]{:S(2)}) collective-permute-start(bf16[128,1536]{1,0:T(8,128)(2,1)S(1)} %collective-permute-done.49.refs_2_), channel_id=1, source_target_pairs={{4,0},{8,4},{12,8},{14,12},{10,14},{6,10},{2,6},{0,2},{5,1},{9,5},... | collective-permute-start | bytes 1179656 | tf_op jit(solution)/shard_map/ppermute | solution.py:301
  462.8 48.1 %collective-permute-start.47 = (bf16[512,1280]{1,0:T(8,128)(2,1)S(1)}, bf16[512,1280]{1,0:T(8,128)(2,1)S(1)}, u32[]{:S(2)}, u32[]{:S(2)}) collective-permute-start(bf16[512,1280]{1,0:T(8,128)(2,1)S(1)} %add_convert_fusion.1), channel_id=1, source_target_pairs={{0,16},{16,0},{1,17},{17,1},{2,18},{18,2},{3,19},{19,3},{4,20},{20... | collective-permute-start | bytes 3932168 | tf_op jit(solution)/shard_map/ppermute | solution.py:318
  467.2 43.6 %collective-permute-start.56 = (bf16[512,768]{1,0:T(8,128)(2,1)S(1)}, bf16[512,768]{1,0:T(8,128)(2,1)S(1)}, u32[]{:S(2)}, u32[]{:S(2)}) collective-permute-start(bf16[512,768]{1,0:T(8,128)(2,1)S(1)} %add_convert_fusion.2), channel_id=1, source_target_pairs={{0,16},{16,0},{1,17},{17,1},{2,18},{18,2},{3,19},{19,3},{4,20},{20... | collective-permute-start | bytes 2359304 | tf_op jit(solution)/shard_map/ppermute | solution.py:318
  (59 other events, 928.3 us)
